TPU v7x, 512 devices: a whole 4x4x16 slice. The times are simulated.
512 devices in a mesh: ep: 32 (over z, core), tp: 16 (over y, x).
Axes of the slice: x: 4, y: 4, z: 16, core: 2. Of those that a mesh axis runs over, the one named last changes fastest.
Arguments:
- query_proj: bfloat16 [16384, 1024], P('ep', 'tp'), may hold values from -6 to 6
- key_proj: bfloat16 [16384, 256], P('ep'), may hold values from -6 to 6
- value_proj: bfloat16 [16384, 256], P('ep'), may hold values from -24 to 24
- sink_logit: float32 [16], P('tp'), may hold values from 2 to 6
- out_weight: bfloat16 [1024, 2048], P(None, 'tp'), may hold values from -0.1875 to 0.1875
- expert_input: bfloat16 [8192, 2048], P('ep'), may hold values from -6 to 6
- norm_gain: float32 [2048], replicated, may hold values from 0.1 to 1.9
- routes: int32 [8192, 2], P('ep'), may hold values from 0 to 31, as said below
- route_weights: float32 [8192, 2], P('ep'), may hold values from 0.2 to 1
- gate_weight: bfloat16 [32, 2048, 4096], P('ep', None, 'tp'), may hold values from -0.125 to 0.125
- up_weight: bfloat16 [32, 2048, 4096], P('ep', None, 'tp'), may hold values from -0.125 to 0.125
- down_weight: bfloat16 [32, 4096, 2048], P('ep', 'tp'), may hold values from -0.09375 to 0.09375
Outputs:
- mixer_out: bfloat16 [16384, 2048], P('ep', 'tp')
- expert_out: bfloat16 [8192, 2048], P('ep', 'tp')
Inputs may be any that keep to these rules, and one draw needn't show every extreme that they name: `routes`: experts form 4 groups of consecutive numbers of equal size. Each row names 2 different experts of one group. In each aligned block of 256 rows no expert is named by more than 32 rows, and in every block some expert is named by exactly 32 rows.
All inputs are finite; a program needn't handle non-finite values.
Results may differ from a plain program's by a relative error of at most 0.017.
Values may be sent and summed in bfloat16 or wider, within the bound.
A program may use at most 64 MiB of HBM per device.

v0:
```python
import jax
import jax.numpy as jnp
from jax import lax
from jax.sharding import Mesh
from jax.sharding import PartitionSpec as P

D = 2048
HEADS = 16
KV_HEADS = 4
HEAD_DIM = 64
HALF_WIN = 128
GROUPS = 4
TOP_K = 2
TP = ("tp_0", "tp_1")


NORM_EPS = 1e-06
ROPE_BASE = 10000.0
NEG_BIG = -1e30


def padded(block, sides, width):
    for axis, dim in sides:
        count = lax.axis_size(axis)
        forward = [(i, i + 1) for i in range(count - 1)]
        backward = [(target, source) for source, target in forward]
        low = lax.ppermute(
            lax.slice_in_dim(block, block.shape[dim] - width, None, axis=dim), axis, forward
        )
        high = lax.ppermute(lax.slice_in_dim(block, 0, width, axis=dim), axis, backward)
        block = jnp.concatenate([low, block, high], axis=dim)
    return block


def in_order(blocks, dim):
    dims = list(blocks.shape[1:])
    dims[dim] *= blocks.shape[0]
    return jnp.moveaxis(blocks, 0, dim).reshape(dims)


def copy_for_each(x, axis):
    devices = lax.axis_size(axis)
    return lax.all_to_all(jnp.broadcast_to(x[None], (devices, *x.shape)), axis, 0, 0, tiled=True)


def collect(x, axis, dim):
    return in_order(copy_for_each(x, axis), dim)


def own_rows(terms, axes):
    so_far = terms.astype(jnp.bfloat16)
    for axis in axes:
        so_far = lax.psum_scatter(so_far, axis, scatter_dimension=0, tiled=True)
    return so_far.astype(jnp.float32)


def rotate(features, position_start):
    count = features.shape[0]
    half_dim = features.shape[-1] // 2
    inverse_freq = 1.0 / ROPE_BASE ** (
        jnp.arange(half_dim, dtype=jnp.float32) * 2.0 / features.shape[-1]
    )
    position = (jnp.arange(count, dtype=jnp.int32) + position_start).astype(jnp.float32)
    angles = position[:, None] * inverse_freq[None, :]
    cosine = jnp.cos(angles)[:, None, :]
    sine_part = jnp.sin(angles)[:, None, :]
    lower_half = features[..., :half_dim]
    upper_half = features[..., half_dim:]
    return jnp.concatenate(
        [
            lower_half * cosine - upper_half * sine_part,
            upper_half * cosine + lower_half * sine_part,
        ],
        axis=-1,
    )


def mixer_half(query_proj, key_proj, value_proj, sink_logit, out_weight):
    row_count = query_proj.shape[0]
    local_heads = query_proj.shape[1] // HEAD_DIM
    per_kv = HEADS // KV_HEADS
    kv_local = max(1, local_heads // per_kv)
    group_size = local_heads // kv_local
    tp_index = lax.axis_index(TP)
    offset = lax.axis_index("ep") * row_count
    seq_total = row_count * lax.axis_size("ep")
    first_kv = tp_index * local_heads // per_kv
    own_keys = lax.dynamic_slice_in_dim(key_proj, first_kv * HEAD_DIM, kv_local * HEAD_DIM, 1)
    own_values = lax.dynamic_slice_in_dim(value_proj, first_kv * HEAD_DIM, kv_local * HEAD_DIM, 1)
    rot_q = rotate(
        query_proj.reshape(row_count, local_heads, HEAD_DIM).astype(jnp.float32), offset
    ).astype(jnp.bfloat16)
    rot_k = rotate(
        own_keys.reshape(row_count, kv_local, HEAD_DIM).astype(jnp.float32), offset
    ).astype(jnp.bfloat16)
    stacked = jnp.stack([rot_k, own_values.reshape(row_count, kv_local, HEAD_DIM)])
    extended = padded(stacked, (("ep", 1),), HALF_WIN)
    own_sink = sink_logit.reshape(kv_local, group_size)
    block_rows = min(512, row_count)
    key_rows = block_rows + 2 * HALF_WIN
    key_offset = jnp.arange(key_rows, dtype=jnp.int32) - HALF_WIN
    key_gap = key_offset[None, :] - jnp.arange(block_rows, dtype=jnp.int32)[:, None]
    query_block = rot_q.reshape(block_rows, kv_local, group_size, HEAD_DIM)
    key_block = extended[0, 0:key_rows]
    value_block = extended[1, 0:key_rows]
    scores = jnp.einsum(
        "qngd,knd->ngqk", query_block, key_block, preferred_element_type=jnp.float32
    ) * HEAD_DIM ** (-0.5)
    global_key = offset + 0 + key_offset
    allowed = (
        (jnp.abs(key_gap) <= HALF_WIN)
        & (global_key >= 0)[None, :]
        & (global_key < seq_total)[None, :]
    )
    scores = jnp.where(allowed[None, None], scores, NEG_BIG)
    row_peak = jnp.maximum(jnp.max(scores, axis=-1), own_sink[:, :, None])
    lifted = jnp.exp(scores - row_peak[..., None])
    norm_total = jnp.sum(lifted, axis=-1) + jnp.exp(own_sink[:, :, None] - row_peak)
    probs = (lifted / norm_total[..., None]).astype(jnp.bfloat16)
    weighted = jnp.einsum("ngqk,knd->qngd", probs, value_block, preferred_element_type=jnp.float32)
    pieces = weighted.astype(jnp.bfloat16).reshape(block_rows, local_heads * HEAD_DIM)
    projected = jnp.dot(collect(pieces, TP, 1), out_weight, preferred_element_type=jnp.float32)
    return projected.astype(jnp.bfloat16)


def expert_half(
    expert_input, norm_gain, routes, route_weights, gate_weight, up_weight, down_weight
):
    row_count = expert_input.shape[0]
    widened = expert_input.astype(jnp.float32)
    normed = (
        widened
        * lax.rsqrt(jnp.mean(widened * widened, axis=1, keepdims=True) + NORM_EPS)
        * norm_gain
    ).astype(jnp.bfloat16)
    local_experts = gate_weight.shape[0]
    ep_count = lax.axis_size("ep")
    expert_count = local_experts * ep_count
    capacity = row_count * GROUPS // expert_count
    col_count = D // lax.axis_size(TP)
    flat_routes = routes.reshape(-1)
    onehot = (flat_routes[:, None] == jnp.arange(expert_count, dtype=jnp.int32)[None, :]).astype(
        jnp.int32
    )
    slot_rank = jnp.sum((jnp.cumsum(onehot, axis=0) - onehot) * onehot, axis=1)
    slot_index = flat_routes * capacity + slot_rank
    source_rows = jnp.arange(row_count * TOP_K, dtype=jnp.int32) // TOP_K
    own_cols = lax.dynamic_slice_in_dim(normed, lax.axis_index(TP) * col_count, col_count, 1)
    outgoing = (
        jnp.zeros((expert_count * capacity, col_count), jnp.bfloat16)
        .at[slot_index]
        .set(own_cols[source_rows])
    )
    arrived = lax.all_to_all(
        outgoing.reshape(expert_count, capacity, col_count),
        "ep",
        split_axis=0,
        concat_axis=1,
        tiled=True,
    )
    shard_piece = collect(arrived, TP, 2)
    gate_sum = jnp.einsum(
        "esd,edh->esh", shard_piece, gate_weight, preferred_element_type=jnp.float32
    )
    up_sum = jnp.einsum("esd,edh->esh", shard_piece, up_weight, preferred_element_type=jnp.float32)
    hidden = (jax.nn.silu(gate_sum) * up_sum).astype(jnp.bfloat16)
    slot_total = hidden.shape[1]
    term = jnp.einsum("esh,ehc->ces", hidden, down_weight, preferred_element_type=jnp.float32)
    summed = own_rows(term.reshape(col_count * lax.axis_size(TP), local_experts * slot_total), TP)
    result = summed.astype(jnp.bfloat16).reshape(col_count, local_experts, ep_count, capacity)
    returned = lax.all_to_all(result, "ep", split_axis=2, concat_axis=1, tiled=True)
    returned = returned.reshape(col_count, expert_count * capacity)
    picked = (
        jnp.take(returned, slot_index, axis=1)
        .reshape(col_count, row_count, TOP_K)
        .astype(jnp.float32)
    )
    combined = jnp.sum(picked * route_weights[None, :, :], axis=2)
    return combined.T.astype(jnp.bfloat16)


def local(
    query_proj,
    key_proj,
    value_proj,
    sink_logit,
    out_weight,
    expert_input,
    norm_gain,
    routes,
    route_weights,
    gate_weight,
    up_weight,
    down_weight,
):
    mixer_out = mixer_half(query_proj, key_proj, value_proj, sink_logit, out_weight)
    expert_out = expert_half(
        expert_input, norm_gain, routes, route_weights, gate_weight, up_weight, down_weight
    )
    return (mixer_out, expert_out)


def solution(mesh):
    finer = Mesh(mesh.devices.reshape(mesh.shape["ep"], 4, 4), ("ep", "tp_0", "tp_1"))
    in_specs = (
        P("ep", TP),
        P("ep", None),
        P("ep", None),
        P(TP),
        P(None, TP),
        P("ep", None),
        P(),
        P("ep", None),
        P("ep", None),
        P("ep", None, TP),
        P("ep", None, TP),
        P("ep", TP, None),
    )
    out_specs = (P("ep", TP), P("ep", TP))
    return jax.shard_map(local, mesh=finer, in_specs=in_specs, out_specs=out_specs, check_vma=False)
```

profile of v0, /device:TPU:1, one launch (start us, length us, event | category | flops | bytes accessed | tf_op | source)
XLA Modules:
  0.0 251.4 jit_solution(438518287984373368)
XLA Ops:
  7.2 0.0 copy-start
  7.2 0.0 reduce-scatter.5.cloned.1.call-start
  7.2 0.0 copy-start.1
  7.2 0.0 copy-start.7
  7.2 1.6 convert_element_type.96
  8.8 0.0 copy-done.1
  8.9 0.3 multiply_reduce_fusion
  9.1 0.0 copy-done.7
  9.1 0.1 copy.41
  9.3 0.1 eq.26
  9.4 0.1 reshape.472
  9.6 1.2 reduce-window.6
  10.8 0.2 slice_reduce_fusion
  11.1 0.1 copy.46
  11.2 0.1 mul.163
  11.4 0.8 dynamic-slice
  12.2 0.1 fusion.47
  12.3 0.1 fusion.34
  12.4 3.1 %scatter_custom_fusion = bf16[1024,128]{1,0:T(8,128)(2,1)S(1)} fusion(s32[512]{0:T(512)S(1)} %bitcast.108, bf16[256,128]{1,0:T(8,128)(2,1)S(1)} %fusion.34, s32[1024]{0:T(1024)S(1)} %pad_clamp_fusion.1, bf16[]{:T(256)} %constant.105.clone.1), kind=kCustom, calls=%fused_computation.59 | custom fusion | bytes 262146 | tf_op jit(solution)/shard_map/scatter | solution.py:152
  15.4 38.8 %all_to_all.28 = bf16[32,32,128]{2,1,0:T(8,128)(2,1)S(1)} all-to-all(bf16[32,32,128]{2,1,0:T(8,128)(2,1)S(1)} %bitcast.103), channel_id=1, replica_groups=mesh['ep'=32,'tp_0'=4,'tp_1'=4] {'ep'}, dimensions={0} | all-to-all | bytes 524288 | tf_op jit(solution)/shard_map/all_to_all | solution.py:154
  54.2 0.1 copy.47
  54.4 0.5 broadcast_in_dim.27
  54.9 0.0 copy-start.9
  54.9 56.5 %all_to_all.29 = bf16[16,1,1024,128]{2,3,1,0:T(8,128)(2,1)S(1)} all-to-all(bf16[16,1,1024,128]{2,3,1,0:T(8,128)(2,1)S(1)} %broadcast_in_dim.27), channel_id=1, replica_groups=mesh['ep'=32,'tp_0'=4,'tp_1'=4] {'tp_0','tp_1'}, dimensions={0} | all-to-all | bytes 8388608 | tf_op jit(solution)/shard_map/all_to_all | solution.py:43
  111.4 2.0 copy-done.2
  113.4 0.0 copy-done.9
  113.4 1.3 fusion.8
  114.6 0.0 copy-done
  114.7 0.0 copy-done.10
  114.7 8.5 %convert_bitcast_fusion = bf16[2048,1024]{0,1:T(8,128)(2,1)} fusion(bf16[1024,2048]{0,1:T(8,128)(2,1)} %bitcast.101, bf16[1,256,2048]{2,1,0:T(8,128)(2,1)S(1)} %copy-done, bf16[1,2048,256]{2,1,0:T(8,128)(2,1)S(1)} %copy-done.10, f32[1024,256]{1,0:T(8,128)S(1)} %fusion.8), kind=kOutput, calls=%fused_computation.3 | convolution fusion | flops 2151153664 | bytes 11534336 | tf_op jit(solution)/shard_map/esh,ehc->ces/dot_general | solution.py:168
  123.2 0.0 reduce-scatter.5.cloned.1.call-update
  123.2 0.0 reduce-scatter.7.cloned.1.call-start
  123.2 0.7 copy-done.4
  124.0 0.1 copy.40
  124.2 0.1 dynamic-slice_bitcast_fusion
  124.3 0.1 bitcast_convert_fusion
  124.4 1.3 fusion.42
  125.7 0.1 pad_maximum_fusion.3
  125.8 3.3 %collective-permute-start = (bf16[2,128,1,64]{3,1,2,0:T(8,128)(2,1)S(1)}, bf16[2,128,1,64]{3,1,2,0:T(8,128)(2,1)S(1)}, u32[]{:S(2)}, u32[]{:S(2)}) collective-permute-start(bf16[2,128,1,64]{3,1,2,0:T(8,128)(2,1)S(1)} %get-tuple-element.2), channel_id=1, source_target_pairs={{0,16},{16,32},{32,48},{48,64},{64,80},{80,96},{96,112},{112,128},... | collective-permute-start | bytes 98312 | tf_op jit(solution)/shard_map/ppermute | solution.py:27
  129.1 2.2 collective-permute-start.1
  131.9 0.0 collective-permute-done
  131.9 3.1 %collective-permute-done.1 = bf16[2,128,1,64]{3,1,2,0:T(8,128)(2,1)S(1)} collective-permute-done((bf16[2,128,1,64]{3,1,2,0:T(8,128)(2,1)S(1)}, bf16[2,128,1,64]{3,1,2,0:T(8,128)(2,1)S(1)}, u32[]{:S(2)}, u32[]{:S(2)}) %collective-permute-start.1) | collective-permute-done | bytes 32800 | tf_op jit(solution)/shard_map/ppermute | solution.py:30
  135.1 0.1 pad_maximum_fusion
  135.2 32.8 %reduce-scatter.5.cloned.1.call-done = bf16[512,1024]{0,1:T(8,128)(2,1)} async-done(((bf16[2048,1024]{0,1:T(8,128)(2,1)}), bf16[512,1024]{0,1:T(8,128)(2,1)}) %reduce-scatter.5.cloned.1.call-update) | async-done | bytes 1048592 | tf_op jit(solution)/shard_map/reduce_scatter | solution.py:53
  168.0 2.3 copy.51
  170.3 0.0 reduce-scatter.7.cloned.1.call-update
  170.3 0.8 fusion.51
  171.2 0.3 fusion.2
  171.4 0.4 fusion.4
  171.8 1.1 broadcast_in_dim.23
  172.9 5.1 %all-to-all-start = ((bf16[16,512,64]{1,2,0:T(8,128)(2,1)}), bf16[16,512,64]{1,2,0:T(8,128)(2,1)S(1)}, u32[]{:S(2)}, u32[]{:S(2)}) async-start(bf16[16,512,64]{1,2,0:T(8,128)(2,1)} %broadcast_in_dim.23), calls=%async_computation | async-start | bytes 2097152 | tf_op jit(solution)/shard_map/all_to_all | solution.py:43
  178.1 25.0 %reduce-scatter.7.cloned.1.call-done = bf16[128,1024]{1,0:T(8,128)(2,1)} async-done(((bf16[512,1024]{1,0:T(8,128)(2,1)}), bf16[128,1024]{1,0:T(8,128)(2,1)}) %reduce-scatter.7.cloned.1.call-update) | async-done | bytes 262160
  203.0 1.8 copy.52
  204.8 0.0 all-to-all-done
  204.8 14.1 %all-to-all-start.3 = ((bf16[128,1,32,32]{0,3,1,2:T(8,128)(2,1)}), bf16[128,1,32,32]{0,3,1,2:T(8,128)(2,1)S(1)}, u32[]{:S(2)}, u32[]{:S(2)}) async-start(bf16[128,1,32,32]{0,3,1,2:T(8,128)(2,1)} %bitcast.36), calls=%async_computation.4 | async-start | bytes 524288 | tf_op jit(solution)/shard_map/all_to_all | solution.py:171
  218.9 0.1 reduce_sum.42
  219.1 0.1 copy.44
  219.1 0.2 copy.45
  219.3 0.0 copy-done.8
  219.3 0.1 copy.50
  219.5 1.1 convolution_convert_fusion
  220.7 20.5 %all-to-all-done.3 = bf16[128,1,32,32]{0,3,1,2:T(8,128)(2,1)S(1)} async-done(((bf16[128,1,32,32]{0,3,1,2:T(8,128)(2,1)}), bf16[128,1,32,32]{0,3,1,2:T(8,128)(2,1)S(1)}, u32[]{:S(2)}, u32[]{:S(2)}) %all-to-all-start.3) | async-done | bytes 262176 | tf_op jit(solution)/shard_map/all_to_all | solution.py:171
  241.2 1.3 gather_fusion
  242.5 2.1 multiply_reduce_fusion.1
  (26 shorter events, 0.2 us)
Async XLA Ops:
  7.2 107.5 %copy-start = (bf16[1,256,2048]{2,1,0:T(8,128)(2,1)S(1)}, bf16[1,256,2048]{2,1,0:T(8,128)(2,1)}, u32[]{:S(2)}) copy-start(bf16[1,256,2048]{2,1,0:T(8,128)(2,1)} %param.23) | copy-start | bytes 3145732
  7.2 160.8 %reduce-scatter.5.cloned.1.call-start = ((), (), s32[]{:S(2)}) async-start(), calls=%async_computation.6 | async-start | bytes 5242880 | tf_op jit(solution)/shard_map/reduce_scatter | solution.py:53
  7.2 1.6 copy-start.1
  7.2 1.9 copy-start.7
  54.9 58.4 %copy-start.9 = (bf16[1,2048,256]{2,1,0:T(8,128)(2,1)S(1)}, bf16[1,2048,256]{2,1,0:T(8,128)(2,1)}, u32[]{:S(2)}) copy-start(bf16[1,2048,256]{2,1,0:T(8,128)(2,1)} %param.21) | copy-start | bytes 3145732
  111.4 2.0 copy-start.2
  113.4 1.3 copy-start.10
  123.2 0.8 copy-start.4
  123.2 1.0 copy-start.5
  123.2 1.1 copy-start.6
  123.2 79.8 %reduce-scatter.7.cloned.1.call-start = ((), (), s32[]{:S(2)}) async-start(), calls=%async_computation.7 | async-start | bytes 1310720
  125.8 6.1 %collective-permute-start = (bf16[2,128,1,64]{3,1,2,0:T(8,128)(2,1)S(1)}, bf16[2,128,1,64]{3,1,2,0:T(8,128)(2,1)S(1)}, u32[]{:S(2)}, u32[]{:S(2)}) collective-permute-start(bf16[2,128,1,64]{3,1,2,0:T(8,128)(2,1)S(1)} %get-tuple-element.2), channel_id=1, source_target_pairs={{0,16},{16,32},{32,48},{48,64},{64,80},{80,96},{96,112},{112,128},... | collective-permute-start | bytes 98312 | tf_op jit(solution)/shard_map/ppermute | solution.py:27
  129.1 6.0 %collective-permute-start.1 = (bf16[2,128,1,64]{3,1,2,0:T(8,128)(2,1)S(1)}, bf16[2,128,1,64]{3,1,2,0:T(8,128)(2,1)S(1)}, u32[]{:S(2)}, u32[]{:S(2)}) collective-permute-start(bf16[2,128,1,64]{3,1,2,0:T(8,128)(2,1)S(1)} %get-tuple-element.3), channel_id=1, source_target_pairs={{16,0},{32,16},{48,32},{64,48},{80,64},{96,80},{112,96},{128,112},... | collective-permute-start | bytes 98312 | tf_op jit(solution)/shard_map/ppermute | solution.py:30
  172.9 46.4 %copy-start.8 = (f32[256,2]{0,1:T(2,128)S(1)}, f32[256,2]{0,1:T(2,128)}, u32[]{:S(2)}) copy-start(f32[256,2]{0,1:T(2,128)} %param.20) | copy-start | bytes 6148
  172.9 46.6 %copy-start.3 = (bf16[1024,128]{1,0:T(8,128)(2,1)S(1)}, bf16[1024,128]{1,0:T(8,128)(2,1)}, u32[]{:S(2)}) copy-start(bf16[1024,128]{1,0:T(8,128)(2,1)} %param.16) | copy-start | bytes 786436
  172.9 31.9 %all-to-all-start = ((bf16[16,512,64]{1,2,0:T(8,128)(2,1)}), bf16[16,512,64]{1,2,0:T(8,128)(2,1)S(1)}, u32[]{:S(2)}, u32[]{:S(2)}) async-start(bf16[16,512,64]{1,2,0:T(8,128)(2,1)} %broadcast_in_dim.23), calls=%async_computation | async-start | bytes 2097152 | tf_op jit(solution)/shard_map/all_to_all | solution.py:43
  204.8 36.3 %all-to-all-start.3 = ((bf16[128,1,32,32]{0,3,1,2:T(8,128)(2,1)}), bf16[128,1,32,32]{0,3,1,2:T(8,128)(2,1)S(1)}, u32[]{:S(2)}, u32[]{:S(2)}) async-start(bf16[128,1,32,32]{0,3,1,2:T(8,128)(2,1)} %bitcast.36), calls=%async_computation.4 | async-start | bytes 524288 | tf_op jit(solution)/shard_map/all_to_all | solution.py:171
Sparse Core Ops, SparseCore 0:
  123.3 44.6 reduce-scatter.4
  170.8 32.1 reduce-scatter.6
where the time goes:
time: 252 us; the launch traced here: 251 us
  blocking collectives  95.3 us (38%)
  waiting for transfers between devices  81.4 us (32%)
  starting transfers between devices  24.7 us (10%)
  local copies, waits for them, and re-layouts  15.5 us (6%)
  between operations  15.1 us (6%)
  matrix products  12.1 us (5%)
  other arithmetic  7.36 us (3%)
    all_to_all x1, blocking collectives, copy_for_each(): lax.all_to_all(jnp.broadcast_to(x[None], (devices, *x.shape)), axis, 0, 0...  56.5 us
    all_to_all x1, blocking collectives, expert_half(): lax.all_to_all(outgoing.reshape(expert_count, capacity, col_count), 'ep',...  38.8 us
    reduce_scatter x1, waiting for transfers between devices, own_rows(): so_far = lax.psum_scatter(so_far, axis, scatter_dimension=0, tiled=True)  32.8 us
    unnamed x3, waiting for transfers between devices  25 us
    all_to_all x1, waiting for transfers between devices, expert_half(): lax.all_to_all(result, 'ep', split_axis=2, concat_axis=1, tiled=True)  20.5 us
    all_to_all x1, starting transfers between devices, expert_half(): lax.all_to_all(result, 'ep', split_axis=2, concat_axis=1, tiled=True)  14.1 us
    dot_general x1, matrix products, expert_half(): jnp.einsum('esh,ehc->ces', hidden, down_weight, preferred_element_type=jn...  8.49 us
    unnamed x27, local copies, waits for them, and re-layouts  7.23 us
  transfers between devices with their start and end apart: 6, of which 4 were waited for; matrix products, arithmetic and copies ran while one was open for 3% of the time, Pallas kernels for 0%

commit v1 on v0

v1 whole, which is shorter than its diff:
```python
import functools

import jax
import jax.numpy as jnp
from jax import lax
from jax.experimental import pallas as pl
from jax.experimental.pallas import tpu as pltpu
from jax.sharding import Mesh
from jax.sharding import PartitionSpec as P

HEADS = 16
KV_HEADS = 4
HEAD_DIM = 64
HALF_WIN = 128
GROUPS = 4
NORM_EPS = 1e-06
ROPE_BASE = 10000.0
NEG_BIG = -1e30
TP = ("tp_0", "tp_1")
SIDE = 4
LANES = 128
PER_UNIT = 4
BF16 = jnp.bfloat16
F32 = jnp.float32
MESH = pl.DeviceIdType.MESH


def padded(block, width):
    count = lax.axis_size("ep")
    forward = [(i, i + 1) for i in range(count - 1)]
    backward = [(target, source) for source, target in forward]
    low = lax.ppermute(block[:, block.shape[1] - width :], "ep", forward)
    high = lax.ppermute(block[:, :width], "ep", backward)
    return jnp.concatenate([low, block, high], axis=1)


def rotate(features, position_start):
    count = features.shape[0]
    half_dim = features.shape[-1] // 2
    inverse_freq = 1.0 / ROPE_BASE ** (
        jnp.arange(half_dim, dtype=F32) * 2.0 / features.shape[-1]
    )
    position = (jnp.arange(count, dtype=jnp.int32) + position_start).astype(F32)
    angles = position[:, None] * inverse_freq[None, :]
    cosine = jnp.cos(angles)
    sine_part = jnp.sin(angles)
    lower_half = features[..., :half_dim]
    upper_half = features[..., half_dim:]
    return jnp.concatenate(
        [
            lower_half * cosine - upper_half * sine_part,
            upper_half * cosine + lower_half * sine_part,
        ],
        axis=-1,
    )


def attend(query_proj, key_proj, value_proj, sink_logit):
    row_count = query_proj.shape[0]
    offset = lax.axis_index("ep") * row_count
    seq_total = row_count * lax.axis_size("ep")
    first_kv = lax.axis_index(TP) // (HEADS // KV_HEADS)
    own_keys = lax.dynamic_slice_in_dim(key_proj, first_kv * HEAD_DIM, HEAD_DIM, 1)
    own_values = lax.dynamic_slice_in_dim(value_proj, first_kv * HEAD_DIM, HEAD_DIM, 1)
    rot_q = rotate(query_proj.astype(F32), offset).astype(BF16)
    rot_k = rotate(own_keys.astype(F32), offset).astype(BF16)
    extended = padded(jnp.stack([rot_k, own_values]), HALF_WIN)
    key_rows = row_count + 2 * HALF_WIN
    key_offset = jnp.arange(key_rows, dtype=jnp.int32) - HALF_WIN
    key_gap = key_offset[None, :] - jnp.arange(row_count, dtype=jnp.int32)[:, None]
    scores = jnp.einsum("qd,kd->qk", rot_q, extended[0], preferred_element_type=F32)
    scores = scores * HEAD_DIM ** (-0.5)
    global_key = offset + key_offset
    allowed = (
        (jnp.abs(key_gap) <= HALF_WIN)
        & (global_key >= 0)[None, :]
        & (global_key < seq_total)[None, :]
    )
    scores = jnp.where(allowed, scores, NEG_BIG)
    row_peak = jnp.maximum(jnp.max(scores, axis=-1), sink_logit[0])
    lifted = jnp.exp(scores - row_peak[:, None])
    norm_total = jnp.sum(lifted, axis=-1) + jnp.exp(sink_logit[0] - row_peak)
    probs = (lifted / norm_total[:, None]).astype(BF16)
    weighted = jnp.einsum("qk,kd->dq", probs, extended[1], preferred_element_type=F32)
    return weighted.astype(BF16)


def exchange_kernel(
    units,
    out_ref,
    att_ref,
    wg_hbm,
    wu_hbm,
    wd_hbm,
    ret_ref,
    atts_ref,
    rows,
    terms,
    transit,
    from_b,
    part,
    from_a,
    result,
    wg,
    wu,
    wd,
    w_sem,
    z_send,
    z_recv,
    ret_send,
    ret_recv,
    ag_send,
    ag_recv,
    rs_send,
    rs_recv,
    att_send,
    att_recv,
):
    ep = lax.axis_index("ep")
    yi = lax.axis_index("tp_0")
    xi = lax.axis_index("tp_1")
    senders = units * PER_UNIT
    chips = senders // 2
    zi = ep // 2
    ci = ep % 2
    cap = out_ref.shape[1]

    def ep_plus(step, flip):
        return ((zi + step) % chips) * 2 + (ci + flip) % 2

    def along_a(par, k):
        return {"tp_0": (yi + k * par) % SIDE, "tp_1": (xi + k * (1 - par)) % SIDE}

    def along_b(par, k):
        return {"tp_0": (yi + k * (1 - par)) % SIDE, "tp_1": (xi + k * par) % SIDE}

    def own_ab(par):
        return xi * (1 - par) + yi * par, yi * (1 - par) + xi * par

    def remote(src, dst, ssem, rsem, dev):
        return pltpu.make_async_remote_copy(
            src_ref=src,
            dst_ref=dst,
            send_sem=ssem,
            recv_sem=rsem,
            device_id=dev,
            device_id_type=MESH,
        )

    loads = [
        pltpu.make_async_copy(src, dst, w_sem.at[i])
        for i, (src, dst) in enumerate(((wg_hbm, wg), (wu_hbm, wu), (wd_hbm, wd)))
    ]
    for load in loads:
        load.start()

    barrier = pltpu.get_barrier_semaphore()
    for j in range(1, senders):
        pl.semaphore_signal(
            barrier, inc=1, device_id={"ep": ep_plus(j // 2, j % 2)}, device_id_type=MESH
        )
    for par in range(2):
        for k in range(1, SIDE):
            pl.semaphore_signal(
                barrier, inc=1, device_id=along_a(par, k), device_id_type=MESH
            )
    pl.semaphore_wait(barrier, senders - 1 + 2 * (SIDE - 1))

    def z_copy(j):
        u, i = j // PER_UNIT, j % PER_UNIT
        a, b = own_ab(u % 2)
        dest = ep_plus(j // 2, j % 2)
        return remote(
            out_ref.at[dest],
            rows.at[u, b, a, pl.ds(i * cap, cap), :],
            z_send.at[j],
            z_recv.at[j],
            {"ep": dest},
        )

    a0, b0 = own_ab(0)
    rows[0, b0, a0, 0:cap, :] = out_ref[ep]
    for j in range(1, senders):
        z_copy(j).start()

    def gather_a(buf, u, par, ssem, rsem):
        a, b = own_ab(par)
        return [
            remote(
                buf.at[u, b, a], buf.at[u, b, a], ssem.at[u, k - 1], rsem.at[u, k - 1], along_a(par, k)
            )
            for k in range(1, SIDE)
        ]

    def gather_a_in(buf, u, par, ssem, rsem):
        a, b = own_ab(par)
        return [
            remote(
                buf.at[u, b, a],
                buf.at[u, b, (a + SIDE - k) % SIDE],
                ssem.at[u, k - 1],
                rsem.at[u, k - 1],
                along_a(par, k),
            )
            for k in range(1, SIDE)
        ]

    def gather_b(buf, u, par, ssem, rsem, back):
        a, b = own_ab(par)
        out = []
        for i, k in enumerate((1, SIDE - 1)):
            at = (b + SIDE - k) % SIDE if back else b
            out.append(
                remote(
                    buf.at[u, b], buf.at[u, at], ssem.at[u, 3 + i], rsem.at[u, 3 + i], along_b(par, k)
                )
            )
        return out

    def gather_c(buf, u, par, ssem, rsem, back):
        a, b = own_ab(par)
        out = []
        for i, k in enumerate((1, SIDE - 1)):
            held = (b + SIDE - k) % SIDE
            at = (b + 2) % SIDE if back else held
            half = pl.ds(2 * i, 2)
            out.append(
                remote(
                    buf.at[u, held, half],
                    buf.at[u, at, half],
                    ssem.at[u, 5 + i],
                    rsem.at[u, 5 + i],
                    along_b(par, k),
                )
            )
        return out

    def start(copies):
        for copy in copies:
            copy.start()

    def arrive(copies):
        for copy in copies:
            copy.wait_recv()

    def sent(copies):
        for copy in copies:
            copy.wait_send()

    rows_sems = (ag_send, ag_recv)
    att_sems = (att_send, att_recv)

    for h in range(2):
        a, b = own_ab(h)
        atts_ref[h, b, a] = att_ref[h]
    for h in range(2):
        a, b = own_ab(h)
        start(gather_a(atts_ref, h, h, *att_sems))

    def reduce_1(u, par, back):
        a, b = own_ab(par)
        out = []
        for i, k in enumerate((1, SIDE - 1)):
            half, rest = pl.ds(2 * i, 2), pl.ds(2 - 2 * i, 2)
            opposite, next_b = (b + 2) % SIDE, (b + k) % SIDE
            out.append(
                remote(
                    terms.at[u, opposite, half],
                    transit.at[u, i],
                    rs_send.at[u, i],
                    rs_recv.at[u, i],
                    along_b(par, k),
                )
            )
            out.append(
                remote(
                    terms.at[u, next_b, rest],
                    from_b.at[u, i, rest],
                    rs_send.at[u, 2 + i],
                    rs_recv.at[u, 2 + i],
                    along_b(par, k),
                )
            )
        return out

    def reduce_2(u, par):
        a, b = own_ab(par)
        out = []
        for i, k in enumerate((1, SIDE - 1)):
            half = pl.ds(2 * i, 2)
            out.append(
                remote(
                    transit.at[u, i],
                    from_b.at[u, i, half],
                    rs_send.at[u, 4 + i],
                    rs_recv.at[u, 4 + i],
                    along_b(par, k),
                )
            )
        return out

    def reduce_3(u, par):
        a, b = own_ab(par)
        return [
            remote(
                part.at[u, (a + k) % SIDE],
                from_a.at[u, k - 1],
                rs_send.at[u, 5 + k],
                rs_recv.at[u, 5 + k],
                along_a(par, k),
            )
            for k in range(1, SIDE)
        ]

    def ret_copy(u, i):
        j = u * PER_UNIT + i
        source = ep_plus(chips - j // 2, j % 2)
        return remote(
            result.at[u, pl.ds(i * cap, cap), :],
            ret_ref.at[ep],
            ret_send.at[j],
            ret_recv.at[j],
            {"ep": source},
        )

    def ret_in(j):
        return remote(
            result.at[0, pl.ds(0, cap), :],
            ret_ref.at[ep_plus(j // 2, j % 2)],
            ret_send.at[j],
            ret_recv.at[j],
            {"ep": ep_plus(j // 2, j % 2)},
        )

    def z_in(j):
        u, i = j // PER_UNIT, j % PER_UNIT
        a, b = own_ab(u % 2)
        return remote(
            out_ref.at[0],
            rows.at[u, b, a, pl.ds(i * cap, cap), :],
            z_send.at[j],
            z_recv.at[j],
            {"ep": ep_plus(chips - j // 2, j % 2)},
        )

    def stage_a0(u):
        par = u % 2
        for i in range(PER_UNIT):
            if i == 0:

                @pl.when(u > 0)
                def _():
                    z_in(u * PER_UNIT).wait_recv()

            else:
                z_in(u * PER_UNIT + i).wait_recv()
        start(gather_a(rows, u, par, *rows_sems))

    def stage_a1(u):
        par = u % 2
        arrive(gather_a_in(rows, u, par, *rows_sems))
        start(gather_b(rows, u, par, *rows_sems, back=False))

    def stage_a2(u):
        par = u % 2
        arrive(gather_b(rows, u, par, *rows_sems, back=True))
        start(gather_c(rows, u, par, *rows_sems, back=False))

    def stage_c(u):
        par = u % 2
        arrive(gather_c(rows, u, par, *rows_sems, back=True))

        @pl.when(u == 0)
        def _():
            for load in loads:
                load.wait()

        def at(t):
            y, x = t // SIDE, t % SIDE
            return y * (1 - par) + x * par, x * (1 - par) + y * par

        blocks = [rows[(u, *at(t))] for t in range(SIDE * SIDE)]
        x = jnp.concatenate(blocks, axis=1)
        gate = jnp.dot(x, wg[...], preferred_element_type=F32)
        up = jnp.dot(x, wu[...], preferred_element_type=F32)
        hidden = (gate / (1.0 + jnp.exp(-gate)) * up).astype(BF16)
        for t in range(SIDE * SIDE):
            term = jnp.dot(
                hidden, wd[:, t * LANES : (t + 1) * LANES], preferred_element_type=F32
            )
            terms[(u, *at(t))] = term.astype(BF16)
        start(reduce_1(u, par, False))

    def stage_r1(u):
        par = u % 2
        a, b = own_ab(par)
        for i, k in enumerate((1, SIDE - 1)):
            half = pl.ds(2 * i, 2)
            reduce_1(u, par, True)[2 * i].wait_recv()
            transit[u, i] = (
                transit[u, i].astype(F32) + terms[u, (b + k) % SIDE, half].astype(F32)
            ).astype(BF16)
            reduce_2(u, par)[i].start()

    def stage_r2(u):
        par = u % 2
        a, b = own_ab(par)
        first = reduce_1(u, par, True)
        arrive([first[1], first[3]])
        arrive(reduce_2(u, par))
        part[u] = (
            terms[u, b].astype(F32) + from_b[u, 0].astype(F32) + from_b[u, 1].astype(F32)
        ).astype(BF16)
        start(reduce_3(u, par))

    def stage_r3(u):
        par = u % 2
        a, b = own_ab(par)
        arrive(reduce_3(u, par))
        total = part[u, a].astype(F32)
        for k in range(SIDE - 1):
            total = total + from_a[u, k].astype(F32)
        result[u] = total.astype(BF16)
        for i in range(PER_UNIT):
            if i == 0:

                @pl.when(u == 0)
                def _():
                    ret_ref[ep] = result[0, 0:cap, :]

                @pl.when(u > 0)
                def _():
                    ret_copy(u, 0).start()

            else:
                ret_copy(u, i).start()

    stages = (
        (6, stage_r3),
        (5, stage_r2),
        (4, stage_r1),
        (2, stage_a2),
        (1, stage_a1),
        (0, stage_a0),
        (3, stage_c),
    )

    def step(s, carry):
        @pl.when(s == 1)
        def _():
            for h in range(2):
                arrive(gather_a_in(atts_ref, h, h, *att_sems))
                start(gather_b(atts_ref, h, h, *att_sems, back=False))

        @pl.when(s == 3)
        def _():
            for h in range(2):
                arrive(gather_b(atts_ref, h, h, *att_sems, back=True))
                start(gather_c(atts_ref, h, h, *att_sems, back=False))

        for lag, stage in stages:

            @pl.when((s >= lag) & (s < units + lag))
            def _(lag=lag, stage=stage):
                stage(s - lag)

        return carry

    lax.fori_loop(0, units + 6, step, 0)

    for h in range(2):
        arrive(gather_c(atts_ref, h, h, *att_sems, back=True))
        sent(gather_a(atts_ref, h, h, *att_sems))
        sent(gather_b(atts_ref, h, h, *att_sems, back=False))
        sent(gather_c(atts_ref, h, h, *att_sems, back=False))

    def drain(u, carry):
        par = u % 2
        sent(gather_a(rows, u, par, *rows_sems))
        sent(gather_b(rows, u, par, *rows_sems, back=False))
        sent(gather_c(rows, u, par, *rows_sems, back=False))
        sent(reduce_1(u, par, False))
        sent(reduce_2(u, par))
        sent(reduce_3(u, par))
        return carry

    lax.fori_loop(0, units, drain, 0)

    def drain_z(j, carry):
        z_copy(j).wait_send()
        ret_copy(j // PER_UNIT, j % PER_UNIT).wait_send()
        ret_in(j).wait_recv()
        return carry

    lax.fori_loop(1, senders, drain_z, 0)


def exchange(outgoing, attended, gate_weight, up_weight, down_weight):
    senders, cap, lanes = outgoing.shape
    units = senders // PER_UNIT
    unit_rows = PER_UNIT * cap
    half = attended.shape[1]
    tokens = attended.shape[2]
    vmem = pl.BlockSpec(memory_space=pltpu.VMEM)
    hbm = pl.BlockSpec(memory_space=pl.ANY)
    block = (unit_rows, lanes)
    dma = pltpu.SemaphoreType.DMA
    return pl.pallas_call(
        functools.partial(exchange_kernel, units),
        out_shape=(
            jax.ShapeDtypeStruct((senders, cap, lanes), BF16),
            jax.ShapeDtypeStruct((2, SIDE, SIDE, half, tokens), BF16),
        ),
        in_specs=[vmem, vmem, hbm, hbm, hbm],
        out_specs=(vmem, vmem),
        scratch_shapes=[
            pltpu.VMEM((units, SIDE, SIDE, *block), BF16),
            pltpu.VMEM((units, SIDE, SIDE, *block), BF16),
            pltpu.VMEM((units, 2, 2, *block), BF16),
            pltpu.VMEM((units, 2, SIDE, *block), BF16),
            pltpu.VMEM((units, SIDE, *block), BF16),
            pltpu.VMEM((units, SIDE - 1, *block), BF16),
            pltpu.VMEM((units, *block), BF16),
            pltpu.VMEM(gate_weight.shape, BF16),
            pltpu.VMEM(up_weight.shape, BF16),
            pltpu.VMEM(down_weight.shape, BF16),
            dma((3,)),
            dma((senders,)),
            dma((senders,)),
            dma((senders,)),
            dma((senders,)),
            dma((units, 7)),
            dma((units, 7)),
            dma((units, 9)),
            dma((units, 9)),
            dma((2, 7)),
            dma((2, 7)),
        ],
        compiler_params=pltpu.CompilerParams(
            collective_id=0, has_side_effects=True, vmem_limit_bytes=56 * 1024 * 1024
        ),
    )(outgoing, attended, gate_weight, up_weight, down_weight)


def local(
    query_proj,
    key_proj,
    value_proj,
    sink_logit,
    out_weight,
    expert_input,
    norm_gain,
    routes,
    route_weights,
    gate_weight,
    up_weight,
    down_weight,
):
    row_count, width = expert_input.shape
    expert_count = gate_weight.shape[0] * lax.axis_size("ep")
    cap = row_count * GROUPS // expert_count
    col_count = width // lax.axis_size(TP)

    widened = expert_input.astype(F32)
    scale = lax.rsqrt(jnp.mean(widened * widened, axis=1, keepdims=True) + NORM_EPS)
    first_col = lax.axis_index(TP) * col_count
    own_cols = lax.dynamic_slice_in_dim(expert_input, first_col, col_count, 1).astype(F32)
    own_gain = lax.dynamic_slice_in_dim(norm_gain, first_col, col_count, 0)
    normed = (own_cols * scale * own_gain).astype(BF16)

    experts = jnp.arange(expert_count, dtype=jnp.int32)
    hot = [(routes[:, k, None] == experts[None, :]) for k in range(2)]
    named = (hot[0] | hot[1]).astype(BF16)
    tokens = jnp.arange(row_count, dtype=jnp.int32)
    earlier = (tokens[None, :] < tokens[:, None]).astype(BF16)
    before = jnp.dot(earlier, named, preferred_element_type=F32)
    slots = [
        routes[:, k] * cap + jnp.sum(jnp.where(hot[k], before, 0.0), axis=1).astype(jnp.int32)
        for k in range(2)
    ]
    slot_ids = jnp.arange(expert_count * cap, dtype=jnp.int32)
    picks = [(slots[k][:, None] == slot_ids[None, :]) for k in range(2)]
    placed = (picks[0] | picks[1]).astype(BF16)
    outgoing = jnp.einsum("rs,rc->sc", placed, normed, preferred_element_type=F32)
    outgoing = outgoing.astype(BF16).reshape(expert_count, cap, col_count)

    attended = attend(query_proj, key_proj, value_proj, sink_logit)
    halves = attended.reshape(2, HEAD_DIM // 2, attended.shape[1])

    returned, gathered = exchange(outgoing, halves, gate_weight[0], up_weight[0], down_weight[0])

    by_head = out_weight.reshape(SIDE, SIDE, 2, HEAD_DIM // 2, out_weight.shape[1])
    first = by_head[:, :, 0]
    second = jnp.swapaxes(by_head[:, :, 1], 0, 1)
    weight = jnp.stack([first, second]).reshape(-1, out_weight.shape[1])
    flat = gathered.reshape(-1, gathered.shape[-1])
    mixer_out = jnp.einsum("fq,fd->qd", flat, weight, preferred_element_type=F32)

    returned = returned.reshape(expert_count * cap, col_count)
    combined = 0.0
    for k in range(2):
        picked = jnp.dot(picks[k].astype(BF16), returned, preferred_element_type=F32)
        combined = combined + picked * route_weights[:, k, None]
    return (mixer_out.astype(BF16), combined.astype(BF16))


def solution(mesh):
    finer = Mesh(mesh.devices.reshape(mesh.shape["ep"], SIDE, SIDE), ("ep", "tp_0", "tp_1"))
    in_specs = (
        P("ep", TP),
        P("ep", None),
        P("ep", None),
        P(TP),
        P(None, TP),
        P("ep", None),
        P(),
        P("ep", None),
        P("ep", None),
        P("ep", None, TP),
        P("ep", None, TP),
        P("ep", TP, None),
    )
    out_specs = (P("ep", TP), P("ep", TP))
    return jax.shard_map(local, mesh=finer, in_specs=in_specs, out_specs=out_specs, check_vma=False)
```

time: 252 us -> 127 us (0.50)
  Pallas kernels: 0 us -> 101 us
  blocking collectives: 95.3 us -> 0 us
  waiting for transfers between devices: 81.4 us -> 0.01 us
  starting transfers between devices: 24.7 us -> 10 us
  between operations: 15.1 us -> 1.55 us
  local copies, waits for them, and re-layouts: 15.5 us -> 2.22 us
  other arithmetic: 7.36 us -> 1.98 us
  matrix products: 12.1 us -> 9.24 us
    pallas_call x0 -> x1, Pallas kernels: none -> 101 us  [exchange(): pl.pallas_call(functools.partial(exchange_kernel, units), out_shape=(jax....]
    all_to_all x2 -> x0, blocking collectives: 95.3 us -> none  [the longest x1 56.5 us: copy_for_each(): lax.all_to_all(jnp.broadcast_to(x[None], (devices, *x.shape)), axis, 0, 0...]
    reduce_scatter x1 -> x0, waiting for transfers between devices: 32.8 us -> none  [own_rows(): so_far = lax.psum_scatter(so_far, axis, scatter_dimension=0, tiled=True)]
    unnamed x3 -> x0, waiting for transfers between devices: 25 us -> none
    all_to_all x2 -> x0, waiting for transfers between devices: 20.5 us -> none  [the longest x1 20.5 us: expert_half(): lax.all_to_all(result, 'ep', split_axis=2, concat_axis=1, tiled=True)]
    all_to_all x2 -> x0, starting transfers between devices: 19.2 us -> none  [the longest x1 14.1 us: expert_half(): lax.all_to_all(result, 'ep', split_axis=2, concat_axis=1, tiled=True)]
    unnamed x27 -> x10, local copies, waits for them, and re-layouts: 7.23 us -> 0.13 us
    ppermute x2, starting transfers between devices: 5.42 us -> 10 us  [the longest x1 5.11 us: padded(): high = lax.ppermute(block[:, :width], 'ep', backward)]
  transfers between devices with their start and end apart: 6 -> 2, of which waited for: 4 -> 0; matrix products, arithmetic and copies ran while one was open for 3% -> 2% of each run, Pallas kernels for 0% -> 0%
where the time goes in v1:
time: 127 us; the launch traced here: 126 us
  Pallas kernels  101 us (80%)
  starting transfers between devices  10 us (8%)
  matrix products  9.24 us (7%)
  local copies, waits for them, and re-layouts  2.22 us (2%)
  other arithmetic  1.98 us (2%)
  between operations  1.55 us (1%)
    pallas_call x1, Pallas kernels, exchange(): pl.pallas_call(functools.partial(exchange_kernel, units), out_shape=(jax....  101 us
    ppermute x1, starting transfers between devices, padded(): high = lax.ppermute(block[:, :width], 'ep', backward)  5.11 us
    ppermute x1, starting transfers between devices, padded(): low = lax.ppermute(block[:, block.shape[1] - width:], 'ep', forward)  4.92 us
    dot_general x2, matrix products, local(): jnp.dot(picks[k].astype(BF16), returned, preferred_element_type=F32)  3.24 us
  transfers between devices with their start and end apart: 2, of which 0 were waited for; matrix products, arithmetic and copies ran while one was open for 2% of the time, Pallas kernels for 0%

profile of v1, /device:TPU:1, one launch (start us, length us, event | category | flops | bytes accessed | tf_op | source)
XLA Modules:
  0.0 126.3 jit_solution(15735297449760599309)
XLA Ops:
  0.6 0.0 copy-start.2
  0.6 0.0 copy-start
  0.7 0.0 copy-start.3
  0.7 0.0 copy-start.1
  0.7 1.2 constant_dynamic-slice_fusion
  1.9 0.1 copy.24
  2.1 0.9 convert_element_type.88
  2.9 0.1 copy.20
  3.0 0.3 fusion.29
  3.4 4.9 %collective-permute-start = (bf16[2,128,64]{1,2,0:T(8,128)(2,1)S(1)}, bf16[2,128,64]{1,2,0:T(8,128)(2,1)S(1)}, u32[]{:S(2)}, u32[]{:S(2)}) collective-permute-start(bf16[2,128,64]{1,2,0:T(8,128)(2,1)S(1)} %get-tuple-element.14), channel_id=1, source_target_pairs={{0,16},{16,32},{32,48},{48,64},{64,80},{80,96},{96,112},{112,128},... | collective-permute-start | bytes 98312 | tf_op jit(solution)/shard_map/ppermute | solution.py:32
  8.3 5.1 %collective-permute-start.1 = (bf16[2,128,64]{1,2,0:T(8,128)(2,1)S(1)}, bf16[2,128,64]{1,2,0:T(8,128)(2,1)S(1)}, u32[]{:S(2)}, u32[]{:S(2)}) collective-permute-start(bf16[2,128,64]{1,2,0:T(8,128)(2,1)S(1)} %get-tuple-element.15), channel_id=1, source_target_pairs={{16,0},{32,16},{48,32},{64,48},{80,64},{96,80},{112,96},{128,112},... | collective-permute-start | bytes 98312 | tf_op jit(solution)/shard_map/ppermute | solution.py:33
  13.5 0.0 copy-done.2
  13.5 0.2 select_reduce_fusion.1
  13.7 0.0 copy-done
  13.7 0.3 multiply_reduce_fusion
  14.0 0.0 copy-done.3
  14.0 0.0 copy-done.1
  14.1 0.8 dynamic_slice.13
  14.8 1.3 %convolution_convert_fusion = bf16[1024,128]{1,0:T(8,128)(2,1)} fusion(s32[256]{0:T(256)S(1)} %bitcast.64, s32[256]{0:T(256)S(1)} %bitcast.66, f32[128]{0:T(128)S(1)} %dynamic_slice.13, f32[256]{0:T(256)S(1)} %add_rsqrt_fusion, bf16[256,2048]{1,0:T(8,128)(2,1)S(1)} %copy-done, s32[]{:T(128)S(6)} %select_n.26), kind=kOutput, calls=%fused_computation.8 | convolution fusion | flops 68157440 | bytes 331268 | tf_op jit(solution)/shard_map/rs,rc->sc/dot_general | solution.py:584
  16.8 0.0 collective-permute-done
  16.8 0.0 collective-permute-done.1
  16.9 0.9 fusion.49
  17.7 0.4 fusion.2
  18.2 1.3 %convolution_convert_fusion.1 = bf16[64,512]{1,0:T(8,128)(2,1)} fusion(f32[512,768]{1,0:T(8,128)S(1)} %get-tuple-element.25, f32[512]{0:T(512)S(1)} %exponential_add_fusion, f32[512]{0:T(512)S(1)} %broadcast_maximum_fusion, bf16[2,768,64]{1,2,0:T(8,128)(2,1)S(1)} %pad_maximum_fusion), kind=kOutput, calls=%fused_computation.15 | convolution fusion | flops 51544064 | bytes 1740800 | tf_op jit(solution)/shard_map/qk,kd->dq/dot_general | solution.py:84
  19.4 101.2 %shard_map.131 = (bf16[32,32,128]{2,1,0:T(8,128)(2,1)}, bf16[2,4,4,32,512]{4,3,2,1,0:T(8,128)(2,1)}) custom-call(bf16[32,32,128]{2,1,0:T(8,128)(2,1)} %bitcast.57, bf16[2,32,512]{2,1,0:T(8,128)(2,1)} %bitcast.59, bf16[2048,256]{1,0:T(8,128)(2,1)} %bitcast.51, bf16[2048,256]{1,0:T(8,128)(2,1)} %bitcast.52, bf16[256,2048]{1,0:T(8,128)(2,1)} %bitcast.53), custom_call_target="tpu_custom_call" | custom-call | tf_op jit(solution)/shard_map/pallas_call | solution.py:508
  120.7 1.3 %convolution_multiply_fusion.1 = f32[256,128]{1,0:T(8,128)S(1)} fusion(bf16[1024,128]{1,0:T(8,128)(2,1)} %bitcast.70, s32[256]{0:T(256)S(1)} %bitcast.67, f32[256]{0:T(256)S(1)} %bitcast.63), kind=kOutput, calls=%fused_computation.13 | convolution fusion | flops 67403776 | bytes 395264 | tf_op jit(solution)/shard_map/dot_general | solution.py:602
  122.0 1.9 %fusion.5 = bf16[256,128]{1,0:T(8,128)(2,1)} fusion(f32[256,128]{1,0:T(8,128)S(1)} %convolution_multiply_fusion.1, bf16[1024,128]{1,0:T(8,128)(2,1)} %bitcast.71, s32[256]{0:T(256)S(1)} %bitcast.65, f32[256]{0:T(256)S(1)} %bitcast.62), kind=kOutput, calls=%fused_computation.14 | convolution fusion | flops 67469312 | bytes 460800 | tf_op jit(solution)/shard_map/dot_general | solution.py:602
  123.9 2.4 %fusion.3 = bf16[512,128]{1,0:T(8,128)(2,1)} fusion(bf16[2,4,4,32,512]{4,3,2,1,0:T(8,128)(2,1)} %get-tuple-element.4, bf16[1,4,4,32,128]{4,3,2,1,0:T(8,128)(2,1)S(1)} %bitcast.58, bf16[1,4,4,32,128]{4,3,2,1,0:T(8,128)(2,1)S(1)} %get-tuple-element.8), kind=kOutput, calls=%fused_computation.10 | convolution fusion | flops 134414336 | bytes 1441792 | tf_op jit(solution)/shard_map/fq,fd->qd/dot_general | solution.py:597
  (17 shorter events, 0.2 us)
Async XLA Ops:
  0.6 12.8 %copy-start.2 = (s32[256,2]{0,1:T(2,128)S(1)}, s32[256,2]{0,1:T(2,128)}, u32[]{:S(2)}) copy-start(s32[256,2]{0,1:T(2,128)} %param.19) | copy-start | bytes 6148
  0.6 13.1 %copy-start = (bf16[256,2048]{1,0:T(8,128)(2,1)S(1)}, bf16[256,2048]{1,0:T(8,128)(2,1)}, u32[]{:S(2)}) copy-start(bf16[256,2048]{1,0:T(8,128)(2,1)} %param.17) | copy-start | bytes 3145732
  0.7 13.3 %copy-start.3 = (f32[256,2]{0,1:T(2,128)S(1)}, f32[256,2]{0,1:T(2,128)}, u32[]{:S(2)}) copy-start(f32[256,2]{0,1:T(2,128)} %param.20) | copy-start | bytes 6148
  0.7 13.3 %copy-start.1 = (bf16[1024,128]{1,0:T(8,128)(2,1)S(1)}, bf16[1024,128]{1,0:T(8,128)(2,1)}, u32[]{:S(2)}) copy-start(bf16[1024,128]{1,0:T(8,128)(2,1)} %param.16) | copy-start | bytes 786436
  3.4 13.4 %collective-permute-start = (bf16[2,128,64]{1,2,0:T(8,128)(2,1)S(1)}, bf16[2,128,64]{1,2,0:T(8,128)(2,1)S(1)}, u32[]{:S(2)}, u32[]{:S(2)}) collective-permute-start(bf16[2,128,64]{1,2,0:T(8,128)(2,1)S(1)} %get-tuple-element.14), channel_id=1, source_target_pairs={{0,16},{16,32},{32,48},{48,64},{64,80},{80,96},{96,112},{112,128},... | collective-permute-start | bytes 98312 | tf_op jit(solution)/shard_map/ppermute | solution.py:32
  8.3 8.5 %collective-permute-start.1 = (bf16[2,128,64]{1,2,0:T(8,128)(2,1)S(1)}, bf16[2,128,64]{1,2,0:T(8,128)(2,1)S(1)}, u32[]{:S(2)}, u32[]{:S(2)}) collective-permute-start(bf16[2,128,64]{1,2,0:T(8,128)(2,1)S(1)} %get-tuple-element.15), channel_id=1, source_target_pairs={{16,0},{32,16},{48,32},{64,48},{80,64},{96,80},{112,96},{128,112},... | collective-permute-start | bytes 98312 | tf_op jit(solution)/shard_map/ppermute | solution.py:33

commit v2 on v0

v2 whole, which is shorter than its diff:
```python
import functools

import jax
import jax.numpy as jnp
from jax import lax
from jax.experimental import pallas as pl
from jax.experimental.pallas import tpu as pltpu
from jax.sharding import Mesh
from jax.sharding import PartitionSpec as P

HEADS = 16
KV_HEADS = 4
HEAD_DIM = 64
HALF_WIN = 128
GROUPS = 4
TOP_K = 2
NORM_EPS = 1e-06
ROPE_BASE = 10000.0
NEG_BIG = -1e30
TP = ("tp_0", "tp_1")
SIDE = 4
LANES = 128
PER_UNIT = 4
BF16 = jnp.bfloat16
F32 = jnp.float32
MESH = pl.DeviceIdType.MESH

Z_ORDER = (0, 1, 2, 3, 9, 4, 10, 11, 12, 5, 6, 7, 13, 8, 14, 15)
Z_ARRIVAL = (0, 2.5, 4, 5.8, 8, 10.5, 13.3, 16.5, 20, 9.2, 10.5, 11.5, 12, 12.4, 12.4, 12)
RELAY = {0: 1, 1: 1, 3: -1, 2: -1}


def plan(units):
    piece, rate, latency = 32.0, 45.56, 2.4
    cost = {"Q": 0.6, "A0": 0.08, "A1": 0.05, "A2": 0.04, "C": 1.0, "P": 0.5}
    cost.update({"R1": 0.15, "R2": 0.3, "R3": 0.25})
    stage = ("Q", "A0", "A1", "A2", "C", "P", "R1", "R2", "R3")
    free, arrival, pending = {}, {}, {}

    def send(now, lanes, size, token, extra=0.0):
        ends = []
        for lane in lanes:
            free[lane] = max(free.get(lane, 0.0), now) + size / rate
            ends.append(free[lane])
        arrival[token] = max(ends) + latency + extra

    per = PER_UNIT // 2
    for u in range(units):
        arrival[("z", u)] = max(Z_ARRIVAL[k] for k in Z_ORDER[u * per : u * per + per])
    for i, ready in enumerate((3.5, 0.0, 0.0, 3.5)):
        arrival[("q", i)] = ready
        pending[("Q", i)] = [("q", i)]
    for u in range(units + 2):
        att = u - units
        first = [("z", u)] if att < 0 else [("Q", 2 * att), ("Q", 2 * att + 1)]
        pending[("A0", u)] = first
        for k in (1, 3, 2):
            pending[("A1", u, k)] = [("a", u, k)]
        for k, s in RELAY.items():
            pending[("A2", u, k)] = [("b", u, k, s)]
        rest = [("b", u, k, s) for k in range(SIDE) for s in (1, -1)]
        rest += [("c", u, k) for k in range(SIDE)]
        pending[("C" if att < 0 else "P", u)] = rest
        if att < 0:
            for i in range(2):
                pending[("R1", u, i)] = [("t", u, i)]
            pending[("R2", u)] = [("f", u, i, j) for i in range(2) for j in range(2)]
            pending[("R3", u)] = [("g", u, k) for k in (1, 2, 3)]

    now, order = 0.0, []
    while pending:
        ready, later = [], []
        for event, needs in pending.items():
            if all(need in arrival for need in needs):
                at = max(arrival[need] for need in needs)
                if at <= now:
                    kind, u = event[0], event[1]
                    place = -1 if kind == "Q" or u >= units else u
                    late = stage.index(kind) >= 4
                    ready.append((late, place, -stage.index(kind), event))
                else:
                    later.append(at)
        if not ready:
            now = min(later)
            continue
        event = min(ready)[-1]
        del pending[event]
        order.append(event)
        kind, u = event[:2]
        now += cost[kind]
        a, b = ("x", "y") if u % 2 == 0 else ("y", "x")
        both = ((a, 1), (a, -1))
        if kind == "Q":
            arrival[event] = now
        elif kind == "A0":
            send(now, both[:1], piece, ("a", u, 1))
            send(now, both[1:], piece, ("a", u, 3))
            send(now, both, piece, ("a", u, 2), 0.7)
        if kind in ("A0", "A1"):
            k = 0 if kind == "A0" else event[2]
            for s in (1, -1):
                send(now, ((b, s),), piece, ("b", u, k, s))
        elif kind == "A2":
            send(now, ((b, RELAY[event[2]]),), piece, ("c", u, event[2]))
        elif kind == "C":
            for i, s in enumerate((1, -1)):
                send(now, ((b, s),), 2 * piece, ("t", u, i))
            for i, s in enumerate((1, -1)):
                send(now, ((b, s),), 2 * piece, ("f", u, i, 0))
        elif kind == "R1":
            send(now, ((b, 1 - 2 * event[2]),), 2 * piece, ("f", u, event[2], 1))
        elif kind == "R2":
            send(now, both[:1], piece, ("g", u, 1))
            send(now, both[1:], piece, ("g", u, 3))
            send(now, both, piece, ("g", u, 2), 0.7)
    return order


def layer_kernel(
    units,
    order,
    query_ref,
    key_ref,
    value_ref,
    freq_ref,
    sink_ref,
    input_ref,
    gain_ref,
    routes_ref,
    weights_ref,
    wo_hbm,
    wg_hbm,
    wu_hbm,
    wd_hbm,
    mixer_ref,
    expert_ref,
    out,
    picks,
    ext,
    rot_q,
    att,
    returned,
    rows,
    terms,
    transit,
    from_b,
    part,
    from_a,
    result,
    wo,
    wg,
    wu,
    wd,
    w_sem,
    halo_send,
    halo_recv,
    z_send,
    z_recv,
    ret_send,
    ret_recv,
    ag_send,
    ag_recv,
    rs_send,
    rs_recv,
):
    ep = lax.axis_index("ep")
    yi = lax.axis_index("tp_0")
    xi = lax.axis_index("tp_1")
    tp = yi * SIDE + xi
    senders = units * PER_UNIT
    chips = senders // 2
    zi = ep // 2
    ci = ep % 2
    cap = out.shape[1]
    tokens = query_ref.shape[0]
    blocks = tokens // HALF_WIN

    def distance(j):
        return Z_ORDER[j // 2]

    def ep_plus(step, flip):
        return ((zi + step) % chips) * 2 + (ci + flip) % 2

    def along_a(par, k):
        return {"tp_0": (yi + k * par) % SIDE, "tp_1": (xi + k * (1 - par)) % SIDE}

    def along_b(par, k):
        return along_a(1 - par, k)

    def own_ab(par):
        return (xi, yi) if par == 0 else (yi, xi)

    def remote(src, dst, ssem, rsem, dev):
        return pltpu.make_async_remote_copy(
            src_ref=src,
            dst_ref=dst,
            send_sem=ssem,
            recv_sem=rsem,
            device_id=dev,
            device_id_type=MESH,
        )

    to_load = ((wg_hbm, wg), (wu_hbm, wu), (wd_hbm, wd), (wo_hbm, wo))
    loads = [pltpu.make_async_copy(s, d, w_sem.at[i]) for i, (s, d) in enumerate(to_load)]
    for load in loads:
        load.start()

    barrier = pltpu.get_barrier_semaphore()
    for j in range(1, senders):
        pl.semaphore_signal(
            barrier, inc=1, device_id={"ep": ep_plus(j // 2, j % 2)}, device_id_type=MESH
        )
    for par in range(2):
        for k in range(1, SIDE):
            pl.semaphore_signal(barrier, inc=1, device_id=along_a(par, k), device_id_type=MESH)

    row_count, width = input_ref.shape
    widened = input_ref[...].astype(F32)
    scale = lax.rsqrt(jnp.mean(widened * widened, axis=1, keepdims=True) + NORM_EPS)
    cols = pl.ds(pl.multiple_of(tp * LANES, LANES), LANES)
    normed = (input_ref[:, cols].astype(F32) * scale * gain_ref[:, cols]).astype(BF16)
    routes = routes_ref[...]
    lane = lax.broadcasted_iota(jnp.int32, (row_count, LANES), 1)
    hot = [routes[:, k : k + 1] == lane for k in range(TOP_K)]
    named = jnp.where(hot[0] | hot[1], 1.0, 0.0).astype(BF16)
    square = (row_count, row_count)
    down, across = (lax.broadcasted_iota(jnp.int32, square, d) for d in range(2))
    earlier = jnp.where(across < down, 1.0, 0.0).astype(BF16)
    before = jnp.dot(earlier, named, preferred_element_type=F32)
    slot_ids = lax.broadcasted_iota(jnp.int32, (row_count, senders * cap), 1)
    for k in range(TOP_K):
        rank = jnp.sum(jnp.where(hot[k], before, 0.0), axis=1, keepdims=True)
        slot = routes[:, k : k + 1] * cap + rank.astype(jnp.int32)
        picks[k] = jnp.where(slot == slot_ids, 1.0, 0.0).astype(BF16)
    placed = picks[0] + picks[1]
    outgoing = lax.dot_general(
        placed, normed, (((0,), (0,)), ((), ())), preferred_element_type=F32
    )
    out[...] = outgoing.astype(BF16).reshape(senders, cap, LANES)

    first_row = ep * tokens
    position = lax.broadcasted_iota(jnp.int32, (tokens, LANES), 0) + first_row
    angles = position.astype(F32) * freq_ref[...]
    cosine, sine = jnp.cos(angles), jnp.sin(angles)

    def selector(depth, first, target, turned):
        shape = (depth, LANES)
        r, c = (lax.broadcasted_iota(jnp.int32, shape, d) for d in range(2))
        inside = (c >= target) & (c < target + HEAD_DIM)
        at = first + c - target
        if not turned:
            return jnp.where(inside & (r == at), 1.0, 0.0).astype(BF16)
        low = c < HEAD_DIM // 2
        half = HEAD_DIM // 2
        sign = jnp.where(low & (r == at + half), -1.0, 0.0)
        sign = sign + jnp.where(~low & (r == at - half), 1.0, 0.0)
        return jnp.where(inside, sign, 0.0).astype(BF16)

    def dot(a, b):
        return jnp.dot(a, b, preferred_element_type=F32)

    depth = key_ref.shape[1]
    own = (tp // (HEADS // KV_HEADS)) * HEAD_DIM
    keys = key_ref[...]
    plain = dot(keys, selector(depth, own, 0, False))
    plain = plain + dot(value_ref[...], selector(depth, own, HEAD_DIM, False))
    turned = dot(keys, selector(depth, own, 0, True))
    ext[HALF_WIN : HALF_WIN + tokens] = (plain * cosine + turned * sine).astype(BF16)
    query = query_ref[...]
    plain = dot(query, selector(HEAD_DIM, 0, 0, False))
    turned = dot(query, selector(HEAD_DIM, 0, 0, True))
    rot_q[...] = (plain * cosine + turned * sine).astype(BF16)

    pl.semaphore_wait(barrier, senders - 1 + 2 * (SIDE - 1))

    def z_copy(j):
        u, i = j // PER_UNIT, j % PER_UNIT
        a, b = own_ab(u % 2)
        dest = ep_plus(distance(j), j % 2)
        return remote(
            out.at[dest],
            rows.at[u, b, a, pl.ds(i * cap, cap), :],
            z_send.at[j],
            z_recv.at[j],
            {"ep": dest},
        )

    def halo_copy(i):
        source = tokens if i == 0 else HALF_WIN
        target = 0 if i == 0 else HALF_WIN + tokens
        return remote(
            ext.at[pl.ds(source, HALF_WIN)],
            ext.at[pl.ds(target, HALF_WIN)],
            halo_send.at[i],
            halo_recv.at[i],
            {"ep": (ep + (1 if i == 0 else senders - 1)) % senders},
        )

    for j in range(1, 4):
        z_copy(j).start()
    for i in range(2):
        halo_copy(i).start()
    for j in range(4, senders):
        z_copy(j).start()
    a0, b0 = own_ab(0)
    rows[0, b0, a0, 0:cap, :] = out[ep]

    def attend(i):
        if i == 0:
            halo_copy(0).wait_recv()
        if i == blocks - 1:
            halo_copy(1).wait_recv()
        near = 3 * HALF_WIN
        window = ext[i * HALF_WIN : i * HALF_WIN + near]
        block_q = rot_q[i * HALF_WIN : (i + 1) * HALF_WIN]
        scores = lax.dot_general(
            block_q, window, (((1,), (1,)), ((), ())), preferred_element_type=F32
        ) * HEAD_DIM ** (-0.5)
        shape = (HALF_WIN, near)
        q_at, k_at = (lax.broadcasted_iota(jnp.int32, shape, d) for d in range(2))
        gap = k_at - q_at
        global_key = first_row + (i - 1) * HALF_WIN + k_at
        allowed = (gap >= 0) & (gap <= 2 * HALF_WIN)
        allowed = allowed & (global_key >= 0) & (global_key < senders * tokens)
        scores = jnp.where(allowed, scores, NEG_BIG)
        sink = sink_ref[...]
        row_peak = jnp.maximum(jnp.max(scores, axis=1, keepdims=True), sink)
        lifted = jnp.exp(scores - row_peak)
        norm_total = jnp.sum(lifted, axis=1, keepdims=True) + jnp.exp(sink - row_peak)
        probs = (lifted / norm_total).astype(BF16)
        weighted = dot(probs, window)
        a, b = own_ab((i // 2) % 2)
        piece_cols = slice((i % 2) * HALF_WIN, (i % 2 + 1) * HALF_WIN)
        att[i // 2, b, a, :, piece_cols] = weighted.T[HEAD_DIM:].astype(BF16)

    def buffer(u):
        return (rows, u) if u < units else (att, u - units)

    def gather_a(u, k, back=False):
        par = u % 2
        a, b = own_ab(par)
        buf, at = buffer(u)
        return remote(
            buf.at[at, b, a],
            buf.at[at, b, (a + SIDE - k) % SIDE if back else a],
            ag_send.at[u, k - 1],
            ag_recv.at[u, k - 1],
            along_a(par, k),
        )

    def gather_b(u, k, s, back=False):
        par = u % 2
        a, b = own_ab(par)
        buf, at = buffer(u)
        col = (a + SIDE - k) % SIDE
        sem = 3 + 2 * k + (0 if s == 1 else 1)
        return remote(
            buf.at[at, b, col],
            buf.at[at, (b + SIDE - s) % SIDE if back else b, col],
            ag_send.at[u, sem],
            ag_recv.at[u, sem],
            along_b(par, s % SIDE),
        )

    def gather_c(u, k, back=False):
        par = u % 2
        a, b = own_ab(par)
        buf, at = buffer(u)
        s = RELAY[k]
        col = (a + SIDE - k) % SIDE
        held = (b + SIDE - s) % SIDE
        return remote(
            buf.at[at, held, col],
            buf.at[at, (b + 2) % SIDE if back else held, col],
            ag_send.at[u, 11 + k],
            ag_recv.at[u, 11 + k],
            along_b(par, s % SIDE),
        )

    turns = ((0, 1), (1, SIDE - 1))

    def reduce_opposite(u, i, k):
        par = u % 2
        a, b = own_ab(par)
        return remote(
            terms.at[u, (b + 2) % SIDE, pl.ds(2 * i, 2)],
            transit.at[u, i],
            rs_send.at[u, i],
            rs_recv.at[u, i],
            along_b(par, k),
        )

    def reduce_next(u, i, k):
        par = u % 2
        a, b = own_ab(par)
        rest = pl.ds(2 - 2 * i, 2)
        return remote(
            terms.at[u, (b + k) % SIDE, rest],
            from_b.at[u, i, rest],
            rs_send.at[u, 2 + i],
            rs_recv.at[u, 2 + i],
            along_b(par, k),
        )

    def reduce_relay(u, i, k):
        return remote(
            transit.at[u, i],
            from_b.at[u, i, pl.ds(2 * i, 2)],
            rs_send.at[u, 4 + i],
            rs_recv.at[u, 4 + i],
            along_b(u % 2, k),
        )

    def reduce_a(u, k):
        a, b = own_ab(u % 2)
        return remote(
            part.at[u, (a + k) % SIDE],
            from_a.at[u, k - 1],
            rs_send.at[u, 5 + k],
            rs_recv.at[u, 5 + k],
            along_a(u % 2, k),
        )

    def ret_copy(j):
        source = ep_plus(chips - distance(j), j % 2)
        return remote(
            result.at[j // PER_UNIT, pl.ds((j % PER_UNIT) * cap, cap), :],
            returned.at[ep],
            ret_send.at[j],
            ret_recv.at[j],
            {"ep": source},
        )

    def gathered(u):
        for k, s in RELAY.items():
            gather_b(u, k, -s, back=True).wait_recv()
            gather_c(u, k, back=True).wait_recv()
        buf, at = buffer(u)
        if u % 2 == 0:
            places = [(t // SIDE, t % SIDE) for t in range(SIDE * SIDE)]
        else:
            places = [(t % SIDE, t // SIDE) for t in range(SIDE * SIDE)]
        return places, [buf[(at, *place)] for place in places]

    loaded = []

    def expert(u):
        places, pieces = gathered(u)
        if not loaded:
            loaded.append(u)
            for load in loads[:3]:
                load.wait()
        x = jnp.concatenate(pieces, axis=1)
        gate = dot(x, wg[...])
        up = dot(x, wu[...])
        hidden = (gate / (1.0 + jnp.exp(-gate)) * up).astype(BF16)
        for t, place in enumerate(places):
            terms[(u, *place)] = dot(hidden, wd[:, t * LANES : (t + 1) * LANES]).astype(BF16)
        for i, k in turns:
            reduce_opposite(u, i, k).start()
        for i, k in turns:
            reduce_next(u, i, k).start()

    projected = []

    def project(u):
        places, pieces = gathered(u)
        if not projected:
            loads[3].wait()
        projected.append(u)
        x = jnp.concatenate(pieces, axis=0)
        half = x.shape[1]
        at = (u - units) * half
        total = lax.dot_general(x, wo[...], (((0,), (0,)), ((), ())), preferred_element_type=F32)
        mixer_ref[at : at + half] = total.astype(BF16)

    for event in order:
        kind, u = event[:2]
        a, b = own_ab(u % 2)
        if kind == "Q":
            attend(u)
        elif kind == "A0":
            if u < units:
                for j in range(u * PER_UNIT, (u + 1) * PER_UNIT):
                    if j:
                        z_copy(j).wait_recv()
            for k in (1, 3, 2):
                gather_a(u, k).start()
            for s in (1, -1):
                gather_b(u, 0, s).start()
        elif kind == "A1":
            k = event[2]
            gather_a(u, k, back=True).wait_recv()
            for s in (1, -1):
                gather_b(u, k, s).start()
        elif kind == "A2":
            k = event[2]
            gather_b(u, k, RELAY[k], back=True).wait_recv()
            gather_c(u, k).start()
        elif kind == "C":
            expert(u)
        elif kind == "P":
            project(u)
        elif kind == "R1":
            i, k = turns[event[2]]
            reduce_opposite(u, i, k).wait_recv()
            held = terms[u, (b + k) % SIDE, 2 * i : 2 * i + 2]
            transit[u, i] = (transit[u, i].astype(F32) + held.astype(F32)).astype(BF16)
            reduce_relay(u, i, k).start()
        elif kind == "R2":
            for i, k in turns:
                reduce_next(u, i, k).wait_recv()
                reduce_relay(u, i, k).wait_recv()
            part[u] = (
                terms[u, b].astype(F32) + from_b[u, 0].astype(F32) + from_b[u, 1].astype(F32)
            ).astype(BF16)
            for k in (1, 3, 2):
                reduce_a(u, k).start()
        elif kind == "R3":
            total = part[u, a].astype(F32)
            for k in (1, 3, 2):
                reduce_a(u, k).wait_recv()
                total = total + from_a[u, k - 1].astype(F32)
            result[u] = total.astype(BF16)
            for j in range(u * PER_UNIT, (u + 1) * PER_UNIT):
                if j:
                    ret_copy(j).start()
                else:
                    returned[ep] = result[0, 0:cap, :]

    for u in range(units + 2):
        for k in (1, 3, 2):
            gather_a(u, k).wait_send()
        for k in range(SIDE):
            for s in (1, -1):
                gather_b(u, k, s).wait_send()
            gather_c(u, k).wait_send()
    for u in range(units):
        for i, k in turns:
            reduce_opposite(u, i, k).wait_send()
            reduce_next(u, i, k).wait_send()
            reduce_relay(u, i, k).wait_send()
        for k in (1, 3, 2):
            reduce_a(u, k).wait_send()
    for i in range(2):
        halo_copy(i).wait_send()
    for j in range(1, senders):
        z_copy(j).wait_send()
    for j in range(1, senders):
        ret_copy(j).wait()
    back = returned[...].reshape(senders * cap, LANES)
    combined = dot(picks[0], back) * weights_ref[:, 0:1]
    combined = combined + dot(picks[1], back) * weights_ref[:, 1:2]
    expert_ref[...] = combined.astype(BF16)


def local(
    query_proj,
    key_proj,
    value_proj,
    sink_logit,
    out_weight,
    expert_input,
    norm_gain,
    routes,
    route_weights,
    gate_weight,
    up_weight,
    down_weight,
):
    row_count, width = expert_input.shape
    tokens = query_proj.shape[0]
    senders = gate_weight.shape[0] * lax.axis_size("ep")
    cap = row_count * GROUPS // senders
    units = senders // PER_UNIT
    half_dim = HEAD_DIM // 2
    inverse_freq = 1.0 / ROPE_BASE ** (jnp.arange(half_dim, dtype=F32) * 2.0 / HEAD_DIM)
    zeros = jnp.zeros((LANES - HEAD_DIM,), F32)
    freq = jnp.concatenate([inverse_freq, inverse_freq, zeros])[None, :]

    vmem = pl.BlockSpec(memory_space=pltpu.VMEM)
    hbm = pl.BlockSpec(memory_space=pl.ANY)
    dma = pltpu.SemaphoreType.DMA
    block = (PER_UNIT * cap, LANES)
    gate, up, down = gate_weight[0], up_weight[0], down_weight[0]
    return pl.pallas_call(
        functools.partial(layer_kernel, units, plan(units)),
        out_shape=(
            jax.ShapeDtypeStruct((tokens, LANES), BF16),
            jax.ShapeDtypeStruct((row_count, LANES), BF16),
        ),
        in_specs=[vmem] * 9 + [hbm] * 4,
        out_specs=(vmem, vmem),
        scratch_shapes=[
            pltpu.VMEM((senders, cap, LANES), BF16),
            pltpu.VMEM((TOP_K, row_count, senders * cap), BF16),
            pltpu.VMEM((tokens + 2 * HALF_WIN, LANES), BF16),
            pltpu.VMEM((tokens, LANES), BF16),
            pltpu.VMEM((2, SIDE, SIDE, HEAD_DIM, tokens // 2), BF16),
            pltpu.VMEM((senders, cap, LANES), BF16),
            pltpu.VMEM((units, SIDE, SIDE, *block), BF16),
            pltpu.VMEM((units, SIDE, SIDE, *block), BF16),
            pltpu.VMEM((units, 2, 2, *block), BF16),
            pltpu.VMEM((units, 2, SIDE, *block), BF16),
            pltpu.VMEM((units, SIDE, *block), BF16),
            pltpu.VMEM((units, SIDE - 1, *block), BF16),
            pltpu.VMEM((units, *block), BF16),
            pltpu.VMEM(out_weight.shape, BF16),
            pltpu.VMEM(gate.shape, BF16),
            pltpu.VMEM(up.shape, BF16),
            pltpu.VMEM(down.shape, BF16),
            dma((4,)),
            dma((2,)),
            dma((2,)),
            dma((senders,)),
            dma((senders,)),
            dma((senders,)),
            dma((senders,)),
            dma((units + 2, 15)),
            dma((units + 2, 15)),
            dma((units, 9)),
            dma((units, 9)),
        ],
        compiler_params=pltpu.CompilerParams(
            collective_id=0, has_side_effects=True, vmem_limit_bytes=56 * 1024 * 1024
        ),
    )(
        query_proj,
        key_proj,
        value_proj,
        freq,
        sink_logit.reshape(1, 1),
        expert_input,
        norm_gain[None, :],
        routes,
        route_weights,
        out_weight,
        gate,
        up,
        down,
    )


def solution(mesh):
    finer = Mesh(mesh.devices.reshape(mesh.shape["ep"], SIDE, SIDE), ("ep", "tp_0", "tp_1"))
    in_specs = (
        P("ep", TP),
        P("ep", None),
        P("ep", None),
        P(TP),
        P(None, TP),
        P("ep", None),
        P(),
        P("ep", None),
        P("ep", None),
        P("ep", None, TP),
        P("ep", None, TP),
        P("ep", TP, None),
    )
    out_specs = (P("ep", TP), P("ep", TP))
    return jax.shard_map(local, mesh=finer, in_specs=in_specs, out_specs=out_specs, check_vma=False)
```

time: 252 us -> 102 us (0.40)
  blocking collectives: 95.3 us -> 0 us
  Pallas kernels: 0 us -> 94.5 us
  waiting for transfers between devices: 81.4 us -> 0 us
  starting transfers between devices: 24.7 us -> 0 us
  between operations: 15.1 us -> 1.31 us
  matrix products: 12.1 us -> 0 us
  local copies, waits for them, and re-layouts: 15.5 us -> 5.42 us
  other arithmetic: 7.36 us -> 0.6 us
    all_to_all x2 -> x0, blocking collectives: 95.3 us -> none  [the longest x1 56.5 us: copy_for_each(): lax.all_to_all(jnp.broadcast_to(x[None], (devices, *x.shape)), axis, 0, 0...]
    pallas_call x0 -> x1, Pallas kernels: none -> 94.5 us  [local(): pl.pallas_call(functools.partial(layer_kernel, units, plan(units)), out_s...]
    reduce_scatter x1 -> x0, waiting for transfers between devices: 32.8 us -> none  [own_rows(): so_far = lax.psum_scatter(so_far, axis, scatter_dimension=0, tiled=True)]
    unnamed x3 -> x0, waiting for transfers between devices: 25 us -> none
    all_to_all x2 -> x0, waiting for transfers between devices: 20.5 us -> none  [the longest x1 20.5 us: expert_half(): lax.all_to_all(result, 'ep', split_axis=2, concat_axis=1, tiled=True)]
    all_to_all x2 -> x0, starting transfers between devices: 19.2 us -> none  [the longest x1 14.1 us: expert_half(): lax.all_to_all(result, 'ep', split_axis=2, concat_axis=1, tiled=True)]
    dot_general x5 -> x0, matrix products: 12.1 us -> none  [the longest x1 8.49 us: expert_half(): jnp.einsum('esh,ehc->ces', hidden, down_weight, preferred_element_type=jn...]
    ppermute x2 -> x0, starting transfers between devices: 5.42 us -> none  [the longest x1 3.26 us: padded(): lax.ppermute(lax.slice_in_dim(block, block.shape[dim] - width, None, axis...]
  transfers between devices with their start and end apart: 6 -> 0, of which waited for: 4 -> 0; matrix products, arithmetic and copies ran while one was open for 3% -> 0% of each run, Pallas kernels for 0% -> 0%
where the time goes in v2:
time: 102 us
  Pallas kernels  94.5 us (93%)
  local copies, waits for them, and re-layouts  5.42 us (5%)
  between operations  1.31 us (1%)
    pallas_call x1, Pallas kernels, local(): pl.pallas_call(functools.partial(layer_kernel, units, plan(units)), out_s...  94.5 us
    unnamed x11, local copies, waits for them, and re-layouts  5.42 us

profile of v2, /device:TPU:1, one launch (start us, length us, event | category | flops | bytes accessed | tf_op | source)
XLA Modules:
  0.0 101.8 jit_solution(9122069533251479081)
XLA Ops:
  1.3 0.6 maximum_bitcast_fusion.freq_ref
  1.9 0.0 copy-start.1
  1.9 1.6 %copy.14.query_ref = bf16[512,64]{1,0:T(8,128)(2,1)} copy(bf16[512,64]{0,1:T(8,128)(2,1)} %param.12) | data formatting | bytes 131072 | tf_op args[0]
  3.5 0.0 copy-done.1
  3.5 0.0 copy-start.2
  3.5 0.8 copy.15.routes_ref
  4.3 0.0 copy-done.2
  4.3 0.8 copy.16.weights_ref
  5.1 94.5 %shard_map.131 = (bf16[512,128]{1,0:T(8,128)(2,1)}, bf16[256,128]{1,0:T(8,128)(2,1)}) custom-call(bf16[512,64]{1,0:T(8,128)(2,1)} %copy.14.query_ref, bf16[512,256]{1,0:T(8,128)(2,1)} %key_ref.1, bf16[512,256]{1,0:T(8,128)(2,1)} %value_ref.1, f32[1,128]{1,0:T(1,128)} %maximum_bitcast_fusion.freq_ref, f32[1,1]{1,0:T(1,128)} %bitcast.7.sink_ref, ...), custom_call_target="tpu_custom_call" | custom-call | tf_op jit(solution)/shard_map/pallas_call | solution.py:586
  99.5 0.0 copy-start
  99.5 1.6 %copy.20 = bf16[512,128]{1,0:T(8,128)(2,1)} copy(bf16[512,128]{1,0:T(8,128)(2,1)} %get-tuple-element.4) | data formatting | bytes 262144
  101.1 0.0 copy-done
  101.2 0.6 copy.21
  (2 shorter events, 0.0 us)
Async XLA Ops:
  1.9 1.6 %copy-start.1 = (s32[256,2]{0,1:T(2,128)S(1)}, s32[256,2]{0,1:T(2,128)}, u32[]{:S(2)}) copy-start(s32[256,2]{0,1:T(2,128)} %param.19) | copy-start | bytes 6148
  3.5 0.8 copy-start.2
  99.5 1.6 %copy-start = (bf16[256,128]{1,0:T(8,128)(2,1)S(1)}, bf16[256,128]{1,0:T(8,128)(2,1)}, u32[]{:S(2)}) copy-start(bf16[256,128]{1,0:T(8,128)(2,1)} %get-tuple-element.5) | copy-start | bytes 196612

commit v3 on v2

--- a/solution.py
+++ b/solution.py
@@ -2,6 +2,7 @@
 
 import jax
 import jax.numpy as jnp
+import numpy as np
 from jax import lax
 from jax.experimental import pallas as pl
 from jax.experimental.pallas import tpu as pltpu
@@ -119,23 +120,24 @@
 def layer_kernel(
     units,
     order,
-    query_ref,
-    key_ref,
-    value_ref,
-    freq_ref,
     sink_ref,
-    input_ref,
-    gain_ref,
-    routes_ref,
-    weights_ref,
-    wo_hbm,
+    input_hbm,
+    gain_hbm,
+    routes_hbm,
+    key_hbm,
+    value_hbm,
+    query_hbm,
+    freq_hbm,
+    weights_hbm,
     wg_hbm,
     wu_hbm,
     wd_hbm,
+    wo_hbm,
     mixer_ref,
     expert_ref,
     out,
     picks,
+    raw,
     ext,
     rot_q,
     att,
@@ -147,11 +149,19 @@
     part,
     from_a,
     result,
-    wo,
+    input_ref,
+    gain_ref,
+    routes_ref,
+    key_ref,
+    value_ref,
+    query_ref,
+    freq_ref,
+    weights_ref,
     wg,
     wu,
     wd,
-    w_sem,
+    wo,
+    load_sem,
     halo_send,
     halo_recv,
     z_send,
@@ -172,7 +182,7 @@
     zi = ep // 2
     ci = ep % 2
     cap = out.shape[1]
-    tokens = query_ref.shape[0]
+    tokens = query_ref.shape[1]
     blocks = tokens // HALF_WIN
 
     def distance(j):
@@ -200,11 +210,6 @@
             device_id_type=MESH,
         )
 
-    to_load = ((wg_hbm, wg), (wu_hbm, wu), (wd_hbm, wd), (wo_hbm, wo))
-    loads = [pltpu.make_async_copy(s, d, w_sem.at[i]) for i, (s, d) in enumerate(to_load)]
-    for load in loads:
-        load.start()
-
     barrier = pltpu.get_barrier_semaphore()
     for j in range(1, senders):
         pl.semaphore_signal(
@@ -214,14 +219,38 @@
         for k in range(1, SIDE):
             pl.semaphore_signal(barrier, inc=1, device_id=along_a(par, k), device_id_type=MESH)
 
-    row_count, width = input_ref.shape
+    to_load = (
+        (input_hbm, input_ref),
+        (gain_hbm, gain_ref),
+        (routes_hbm, routes_ref),
+        (key_hbm, key_ref),
+        (value_hbm, value_ref),
+        (query_hbm, query_ref),
+        (freq_hbm, freq_ref),
+        (weights_hbm, weights_ref),
+        (wg_hbm, wg),
+        (wu_hbm, wu),
+        (wd_hbm, wd),
+        (wo_hbm, wo),
+    )
+    loads = [pltpu.make_async_copy(s, d, load_sem.at[i]) for i, (s, d) in enumerate(to_load)]
+    for load in loads:
+        load.start()
+
+    def upright(row):
+        return jnp.broadcast_to(row, (LANES, row.shape[1])).T
+
+    row_count = input_ref.shape[0]
+    for load in loads[:3]:
+        load.wait()
     widened = input_ref[...].astype(F32)
     scale = lax.rsqrt(jnp.mean(widened * widened, axis=1, keepdims=True) + NORM_EPS)
     cols = pl.ds(pl.multiple_of(tp * LANES, LANES), LANES)
     normed = (input_ref[:, cols].astype(F32) * scale * gain_ref[:, cols]).astype(BF16)
-    routes = routes_ref[...]
-    lane = lax.broadcasted_iota(jnp.int32, (row_count, LANES), 1)
-    hot = [routes[:, k : k + 1] == lane for k in range(TOP_K)]
+    routes = routes_ref[...].astype(F32)
+    named_by = [upright(routes[k : k + 1]) for k in range(TOP_K)]
+    lane = lax.broadcasted_iota(jnp.int32, (row_count, LANES), 1).astype(F32)
+    hot = [named_by[k] == lane for k in range(TOP_K)]
     named = jnp.where(hot[0] | hot[1], 1.0, 0.0).astype(BF16)
     square = (row_count, row_count)
     down, across = (lax.broadcasted_iota(jnp.int32, square, d) for d in range(2))
@@ -230,7 +259,7 @@
     slot_ids = lax.broadcasted_iota(jnp.int32, (row_count, senders * cap), 1)
     for k in range(TOP_K):
         rank = jnp.sum(jnp.where(hot[k], before, 0.0), axis=1, keepdims=True)
-        slot = routes[:, k : k + 1] * cap + rank.astype(jnp.int32)
+        slot = (named_by[k][:, 0:1] * cap + rank).astype(jnp.int32)
         picks[k] = jnp.where(slot == slot_ids, 1.0, 0.0).astype(BF16)
     placed = picks[0] + picks[1]
     outgoing = lax.dot_general(
@@ -239,9 +268,6 @@
     out[...] = outgoing.astype(BF16).reshape(senders, cap, LANES)
 
     first_row = ep * tokens
-    position = lax.broadcasted_iota(jnp.int32, (tokens, LANES), 0) + first_row
-    angles = position.astype(F32) * freq_ref[...]
-    cosine, sine = jnp.cos(angles), jnp.sin(angles)
 
     def selector(depth, first, target, turned):
         shape = (depth, LANES)
@@ -259,17 +285,13 @@
     def dot(a, b):
         return jnp.dot(a, b, preferred_element_type=F32)
 
+    for load in loads[3:5]:
+        load.wait()
     depth = key_ref.shape[1]
     own = (tp // (HEADS // KV_HEADS)) * HEAD_DIM
-    keys = key_ref[...]
-    plain = dot(keys, selector(depth, own, 0, False))
+    plain = dot(key_ref[...], selector(depth, own, 0, False))
     plain = plain + dot(value_ref[...], selector(depth, own, HEAD_DIM, False))
-    turned = dot(keys, selector(depth, own, 0, True))
-    ext[HALF_WIN : HALF_WIN + tokens] = (plain * cosine + turned * sine).astype(BF16)
-    query = query_ref[...]
-    plain = dot(query, selector(HEAD_DIM, 0, 0, False))
-    turned = dot(query, selector(HEAD_DIM, 0, 0, True))
-    rot_q[...] = (plain * cosine + turned * sine).astype(BF16)
+    raw[HALF_WIN : HALF_WIN + tokens] = plain.astype(BF16)
 
     pl.semaphore_wait(barrier, senders - 1 + 2 * (SIDE - 1))
 
@@ -289,8 +311,8 @@
         source = tokens if i == 0 else HALF_WIN
         target = 0 if i == 0 else HALF_WIN + tokens
         return remote(
-            ext.at[pl.ds(source, HALF_WIN)],
-            ext.at[pl.ds(target, HALF_WIN)],
+            raw.at[pl.ds(source, HALF_WIN)],
+            raw.at[pl.ds(target, HALF_WIN)],
             halo_send.at[i],
             halo_recv.at[i],
             {"ep": (ep + (1 if i == 0 else senders - 1)) % senders},
@@ -305,11 +327,41 @@
     a0, b0 = own_ab(0)
     rows[0, b0, a0, 0:cap, :] = out[ep]
 
+    for load in loads[5:7]:
+        load.wait()
+
+    def turn_table(first, count):
+        position = lax.broadcasted_iota(jnp.int32, (count, LANES), 0) + (first_row + first)
+        angles = position.astype(F32) * freq_ref[...]
+        return jnp.cos(angles), jnp.sin(angles)
+
+    def rotate_keys(first, count, table):
+        cosine, sine = table
+        held = raw[HALF_WIN + first : HALF_WIN + first + count]
+        turned = dot(held, selector(LANES, 0, 0, True))
+        turned = held.astype(F32) * cosine + turned * sine
+        ext[HALF_WIN + first : HALF_WIN + first + count] = turned.astype(BF16)
+
+    table = turn_table(0, tokens)
+    rotate_keys(0, tokens, table)
+
+    def query_dot(turned):
+        return lax.dot_general(
+            query_ref[...],
+            selector(HEAD_DIM, 0, 0, turned),
+            (((0,), (0,)), ((), ())),
+            preferred_element_type=F32,
+        )
+
+    rot_q[...] = (query_dot(False) * table[0] + query_dot(True) * table[1]).astype(BF16)
+
     def attend(i):
         if i == 0:
             halo_copy(0).wait_recv()
+            rotate_keys(-HALF_WIN, HALF_WIN, turn_table(-HALF_WIN, HALF_WIN))
         if i == blocks - 1:
             halo_copy(1).wait_recv()
+            rotate_keys(tokens, HALF_WIN, turn_table(tokens, HALF_WIN))
         near = 3 * HALF_WIN
         window = ext[i * HALF_WIN : i * HALF_WIN + near]
         block_q = rot_q[i * HALF_WIN : (i + 1) * HALF_WIN]
@@ -448,7 +500,7 @@
         places, pieces = gathered(u)
         if not loaded:
             loaded.append(u)
-            for load in loads[:3]:
+            for load in loads[8:11]:
                 load.wait()
         x = jnp.concatenate(pieces, axis=1)
         gate = dot(x, wg[...])
@@ -466,7 +518,7 @@
     def project(u):
         places, pieces = gathered(u)
         if not projected:
-            loads[3].wait()
+            loads[11].wait()
         projected.append(u)
         x = jnp.concatenate(pieces, axis=0)
         half = x.shape[1]
@@ -546,11 +598,13 @@
         halo_copy(i).wait_send()
     for j in range(1, senders):
         z_copy(j).wait_send()
+    loads[7].wait()
+    weights = [upright(weights_ref[k : k + 1]) for k in range(TOP_K)]
     for j in range(1, senders):
         ret_copy(j).wait()
     back = returned[...].reshape(senders * cap, LANES)
-    combined = dot(picks[0], back) * weights_ref[:, 0:1]
-    combined = combined + dot(picks[1], back) * weights_ref[:, 1:2]
+    combined = dot(picks[0], back) * weights[0]
+    combined = combined + dot(picks[1], back) * weights[1]
     expert_ref[...] = combined.astype(BF16)
 
 
@@ -573,27 +627,42 @@
     senders = gate_weight.shape[0] * lax.axis_size("ep")
     cap = row_count * GROUPS // senders
     units = senders // PER_UNIT
-    half_dim = HEAD_DIM // 2
-    inverse_freq = 1.0 / ROPE_BASE ** (jnp.arange(half_dim, dtype=F32) * 2.0 / HEAD_DIM)
-    zeros = jnp.zeros((LANES - HEAD_DIM,), F32)
-    freq = jnp.concatenate([inverse_freq, inverse_freq, zeros])[None, :]
+    steps = np.arange(HEAD_DIM // 2, dtype=np.float32) * np.float32(2.0 / HEAD_DIM)
+    inverse_freq = np.float32(1.0) / np.float32(ROPE_BASE) ** steps
+    zeros = np.zeros(LANES - HEAD_DIM, np.float32)
+    freq = np.concatenate([inverse_freq, inverse_freq, zeros])[None, :]
 
     vmem = pl.BlockSpec(memory_space=pltpu.VMEM)
     hbm = pl.BlockSpec(memory_space=pl.ANY)
     dma = pltpu.SemaphoreType.DMA
     block = (PER_UNIT * cap, LANES)
     gate, up, down = gate_weight[0], up_weight[0], down_weight[0]
+    operands = (
+        expert_input,
+        norm_gain[None, :],
+        routes.T,
+        key_proj,
+        value_proj,
+        query_proj.T,
+        jnp.asarray(freq),
+        route_weights.T,
+        gate,
+        up,
+        down,
+        out_weight,
+    )
     return pl.pallas_call(
         functools.partial(layer_kernel, units, plan(units)),
         out_shape=(
             jax.ShapeDtypeStruct((tokens, LANES), BF16),
             jax.ShapeDtypeStruct((row_count, LANES), BF16),
         ),
-        in_specs=[vmem] * 9 + [hbm] * 4,
+        in_specs=[vmem] + [hbm] * len(operands),
         out_specs=(vmem, vmem),
         scratch_shapes=[
             pltpu.VMEM((senders, cap, LANES), BF16),
             pltpu.VMEM((TOP_K, row_count, senders * cap), BF16),
+            pltpu.VMEM((tokens + 2 * HALF_WIN, LANES), BF16),
             pltpu.VMEM((tokens + 2 * HALF_WIN, LANES), BF16),
             pltpu.VMEM((tokens, LANES), BF16),
             pltpu.VMEM((2, SIDE, SIDE, HEAD_DIM, tokens // 2), BF16),
@@ -605,11 +674,8 @@
             pltpu.VMEM((units, SIDE, *block), BF16),
             pltpu.VMEM((units, SIDE - 1, *block), BF16),
             pltpu.VMEM((units, *block), BF16),
-            pltpu.VMEM(out_weight.shape, BF16),
-            pltpu.VMEM(gate.shape, BF16),
-            pltpu.VMEM(up.shape, BF16),
-            pltpu.VMEM(down.shape, BF16),
-            dma((4,)),
+            *(pltpu.VMEM(x.shape, x.dtype) for x in operands),
+            dma((len(operands),)),
             dma((2,)),
             dma((2,)),
             dma((senders,)),
@@ -624,21 +690,7 @@
         compiler_params=pltpu.CompilerParams(
             collective_id=0, has_side_effects=True, vmem_limit_bytes=56 * 1024 * 1024
         ),
-    )(
-        query_proj,
-        key_proj,
-        value_proj,
-        freq,
-        sink_logit.reshape(1, 1),
-        expert_input,
-        norm_gain[None, :],
-        routes,
-        route_weights,
-        out_weight,
-        gate,
-        up,
-        down,
-    )
+    )(sink_logit.reshape(1, 1), *operands)
 
 
 def solution(mesh):

time: 102 us -> 96.5 us (0.946)
  local copies, waits for them, and re-layouts: 5.42 us -> 2.23 us
  Pallas kernels: 94.5 us -> 92.9 us
    unnamed x11 -> x4, local copies, waits for them, and re-layouts: 5.42 us -> 2.23 us
    pallas_call x1, Pallas kernels: 94.5 us -> 92.9 us  [local(): pl.pallas_call(functools.partial(layer_kernel, units, plan(units)), out_s...]
where the time goes in v3:
time: 96.5 us; the launch traced here: 96.4 us
  Pallas kernels  92.9 us (96%)
  local copies, waits for them, and re-layouts  2.23 us (2%)
  between operations  1.3 us (1%)
    pallas_call x1, Pallas kernels, local(): pl.pallas_call(functools.partial(layer_kernel, units, plan(units)), out_s...  92.9 us
    unnamed x4, local copies, waits for them, and re-layouts  2.23 us

profile of v3, /device:TPU:1, one launch (start us, length us, event | category | flops | bytes accessed | tf_op | source)
XLA Modules:
  0.0 96.4 jit_solution(14759870087920937692)
XLA Ops:
  1.3 92.9 %shard_map.140 = (bf16[512,128]{1,0:T(8,128)(2,1)}, bf16[256,128]{1,0:T(8,128)(2,1)}) custom-call(f32[1,1]{1,0:T(1,128)} %bitcast.8.sink_ref, bf16[256,2048]{1,0:T(8,128)(2,1)} %input_hbm.1, f32[1,2048]{1,0:T(1,128)} %bitcast.13, s32[2,256]{1,0:T(2,128)} %bitcast.14, bf16[512,256]{1,0:T(8,128)(2,1)} %key_hbm.1, bf16[512,256]{1,0:T(8,128)(2,1)} %value_hbm.1, ...), custom_call_target="tpu_custom_call" | custom-call | tf_op jit(solution)/shard_map/pallas_call | solution.py:654
  94.1 0.0 copy-start
  94.2 1.6 %copy.18 = bf16[512,128]{1,0:T(8,128)(2,1)} copy(bf16[512,128]{1,0:T(8,128)(2,1)} %get-tuple-element.4) | data formatting | bytes 262144
  95.8 0.0 copy-done
  95.8 0.6 copy.19
Async XLA Ops:
  94.1 1.6 %copy-start = (bf16[256,128]{1,0:T(8,128)(2,1)S(1)}, bf16[256,128]{1,0:T(8,128)(2,1)}, u32[]{:S(2)}) copy-start(bf16[256,128]{1,0:T(8,128)(2,1)} %get-tuple-element.5) | copy-start | bytes 196612

commit v4 on v3

--- a/solution.py
+++ b/solution.py
@@ -26,8 +26,8 @@
 F32 = jnp.float32
 MESH = pl.DeviceIdType.MESH
 
-Z_ORDER = (0, 1, 2, 3, 9, 4, 10, 11, 12, 5, 6, 7, 13, 8, 14, 15)
-Z_ARRIVAL = (0, 2.5, 4, 5.8, 8, 10.5, 13.3, 16.5, 20, 9.2, 10.5, 11.5, 12, 12.4, 12.4, 12)
+Z_ORDER = (0, 2, 14, 3, 9, 7, 8, 10, 6, 11, 12, 5, 4, 13, 1, 15)
+Z_ARRIVAL = (0, 13, 3, 4.5, 15, 14, 12.5, 10, 12.5, 9.5, 11.5, 12.6, 13, 13.2, 3, 13)
 RELAY = {0: 1, 1: 1, 3: -1, 2: -1}
 
 

time: 96.5 us -> 95.6 us (level)
  no operation moved by 1% of the time
where the time goes in v4:
time: 95.6 us; the launch traced here: 95.5 us
  Pallas kernels  92 us (96%)
  local copies, waits for them, and re-layouts  2.23 us (2%)
  between operations  1.3 us (1%)
    pallas_call x1, Pallas kernels, local(): pl.pallas_call(functools.partial(layer_kernel, units, plan(units)), out_s...  92 us
    unnamed x4, local copies, waits for them, and re-layouts  2.23 us

profile of v4, /device:TPU:1, one launch (start us, length us, event | category | flops | bytes accessed | tf_op | source)
XLA Modules:
  0.0 95.5 jit_solution(16675448583841103614)
XLA Ops:
  1.3 92.0 %shard_map.140 = (bf16[512,128]{1,0:T(8,128)(2,1)}, bf16[256,128]{1,0:T(8,128)(2,1)}) custom-call(f32[1,1]{1,0:T(1,128)} %bitcast.8.sink_ref, bf16[256,2048]{1,0:T(8,128)(2,1)} %input_hbm.1, f32[1,2048]{1,0:T(1,128)} %bitcast.13, s32[2,256]{1,0:T(2,128)} %bitcast.14, bf16[512,256]{1,0:T(8,128)(2,1)} %key_hbm.1, bf16[512,256]{1,0:T(8,128)(2,1)} %value_hbm.1, ...), custom_call_target="tpu_custom_call" | custom-call | tf_op jit(solution)/shard_map/pallas_call | solution.py:654
  93.3 0.0 copy-start
  93.3 1.6 %copy.18 = bf16[512,128]{1,0:T(8,128)(2,1)} copy(bf16[512,128]{1,0:T(8,128)(2,1)} %get-tuple-element.4) | data formatting | bytes 262144
  94.9 0.0 copy-done
  94.9 0.6 copy.19
Async XLA Ops:
  93.3 1.6 %copy-start = (bf16[256,128]{1,0:T(8,128)(2,1)S(1)}, bf16[256,128]{1,0:T(8,128)(2,1)}, u32[]{:S(2)}) copy-start(bf16[256,128]{1,0:T(8,128)(2,1)} %get-tuple-element.5) | copy-start | bytes 196612
